TPU v7x, 1024 devices: a whole 4x8x16 slice. The times are simulated.
1024 devices in a mesh: rep: 2 (over z_hi), fs: 64 (over z_lo, y), tp: 8 (over x, core).
Axes of the slice: x: 4, y: 8, z: 16 (z_hi: 2, z_lo: 8; z = z_hi * 8 + z_lo), core: 2. Of those that a mesh axis runs over, the one named last changes fastest.
Arguments:
- stream: bfloat16 [32768, 1536], P(('rep', 'fs')), may hold values from -6 to 6
- mix_pre_gain: float32 [1536], replicated, may hold values from 0.1 to 1.9
- w_outer_gate: bfloat16 [1536, 768], P('fs', 'tp'), may hold values from -0.15625 to 0.15625
- w_inner_gate: bfloat16 [1536, 768], P('fs', 'tp'), may hold values from -0.15625 to 0.15625
- w_value: bfloat16 [1536, 768], P('fs', 'tp'), may hold values from -0.15625 to 0.15625
- mix_taps: float32 [3, 768], P(None, 'tp'), may hold values from -3 to 3
- w_mix_out: bfloat16 [768, 1536], P('tp', 'fs'), may hold values from -0.625 to 0.625
- mix_post_gain: float32 [1536], replicated, may hold values from 0.1 to 1.9
- ffn_pre_gain: float32 [1536], replicated, may hold values from 0.1 to 1.9
- w_linear: bfloat16 [1536, 4224], P('fs', 'tp'), may hold values from -0.15625 to 0.15625
- w_gated: bfloat16 [1536, 4224], P('fs', 'tp'), may hold values from -0.15625 to 0.15625
- ffn_taps: float32 [3, 4224], P(None, 'tp'), may hold values from -3 to 3
- ffn_bias: float32 [4224], P('tp'), may hold values from -3 to 3
- w_down: bfloat16 [4224, 1536], P('tp', 'fs'), may hold values from -0.25 to 0.25
- ffn_post_gain: float32 [1536], replicated, may hold values from 0.1 to 1.9
Outputs:
- result: bfloat16 [32768, 1536], P(('rep', 'fs'))
All inputs are finite; a program needn't handle non-finite values.
Results may differ from a plain program's by a relative error of at most 0.023.
Values may be sent and summed in bfloat16 or wider, within the bound.
No kernel may reach another device: no remote copies, remote signals or barrier semaphores. Data moves between devices by JAX's collectives and lax.ppermute only.
A program may use at most 64 MiB of HBM per device.

v0:
```python
import jax
import jax.numpy as jnp
from jax import lax
from jax.sharding import Mesh
from jax.sharding import PartitionSpec as P

SEQ_LEN = 128
FS = ("fs_0", "fs_1")
TP = ("x", "core")
REP_FS = ("rep", "fs_0", "fs_1")
EPS = 1e-06
F32 = jnp.float32
BF16 = jnp.bfloat16


def from_ahead(x, steps):
    n = lax.axis_size("rep") * lax.axis_size("fs_0")
    return lax.ppermute(x, ("rep", "fs_0"), [(i, (i - steps) % n) for i in range(n)])


def doubled(x, sign):
    n = lax.axis_size("fs_0")
    offsets, step = [0], n // 2
    while step:
        arrived = from_ahead(x, sign * step)
        x = jnp.concatenate([x, arrived], axis=0)
        offsets += [o + sign * step for o in offsets]
        step //= 2
    return x, [o % n for o in offsets]


def other_core(x):
    return lax.ppermute(x, "core", [(0, 1), (1, 0)])


def norm_scale(values, gain):
    return values * lax.rsqrt(jnp.mean(values * values, axis=-1, keepdims=True) + EPS) * gain


def conv_three(values, taps):
    height, breadth = values.shape
    grouped = values.reshape(height // SEQ_LEN, SEQ_LEN, breadth)
    padded = jnp.pad(grouped, ((0, 0), (1, 1), (0, 0)))
    mixed = taps[0] * padded[:, :-2] + taps[1] * padded[:, 1:-1] + taps[2] * padded[:, 2:]
    return mixed.reshape(height, breadth)


def dot(a, b):
    return jnp.dot(a, b, preferred_element_type=F32)


def dot_t(a, b):
    return lax.dot_general(a, b, (((1,), (1,)), ((), ())), preferred_element_type=F32)


def sent_to_all(x, axis):
    n = lax.axis_size(axis)
    tiles = lax.all_to_all(jnp.broadcast_to(x[None], (n, *x.shape)), axis, 0, 0, tiled=True)
    return tiles.reshape(-1, x.shape[1])


def rows_summed(partial_value):
    n = lax.axis_size("x")
    tiles = partial_value.astype(BF16).reshape(n, -1, partial_value.shape[1])
    arrived = lax.all_to_all(tiles, "x", split_axis=0, concat_axis=0, tiled=True)
    return arrived.astype(F32).sum(axis=0).astype(BF16).astype(F32)


def layer(
    stream,
    mix_pre_gain,
    w_outer_gate,
    w_inner_gate,
    w_value,
    mix_taps,
    w_mix_out,
    mix_post_gain,
    ffn_pre_gain,
    w_linear,
    w_gated,
    ffn_taps,
    ffn_bias,
    w_down,
    ffn_post_gain,
):
    width = w_value.shape[1]
    hidden_w = w_linear.shape[1]
    rows = w_value.shape[0]
    n0, n1 = lax.axis_size("fs_0"), lax.axis_size("fs_1")
    d = stream.shape[1]
    core = lax.axis_index("core")

    ffn_cols = jnp.concatenate([w_linear, w_gated, w_down.T], axis=1)
    ffn_part, offsets = doubled(ffn_cols, 1)
    ffn_full = lax.all_gather(ffn_part, ("core", "fs_1"), axis=0, tiled=True)
    ffn_full = [ffn_full[:d], ffn_full[d:]]

    mix_cols = jnp.concatenate([w_outer_gate, w_inner_gate, w_value, w_mix_out.T], axis=1)
    mix_part = sent_to_all(mix_cols, "fs_1")
    mix_part, back = doubled(mix_part, -1)
    mix_part = mix_part.reshape(n0, n1, rows, mix_cols.shape[1])
    mix_own = jnp.stack([mix_part[back.index(o)] for o in offsets], axis=1).reshape(d, -1)
    mix_full = [mix_own, other_core(mix_own)]

    small = jnp.concatenate(
        [ffn_taps, ffn_bias[None], jnp.pad(mix_taps, ((0, 0), (0, hidden_w - width)))], axis=0
    )
    small = [small, other_core(small)]
    mix_taps = [s[4:7, :width] for s in small]
    small = [jnp.where(core == 0, small[0], small[1]), jnp.where(core == 0, small[1], small[0])]

    place = jnp.arange(d)
    k = place // rows % n0
    ahead = sum(jnp.where(k == i, o, 0) for i, o in enumerate(offsets))
    z = (lax.axis_index("fs_0") + ahead) % n0
    source = z * (n1 * rows) + place // (rows * n0) * rows + place % rows
    chosen = (jnp.arange(d)[:, None] == source[None, :]).astype(BF16)

    def turned(gain):
        blocks = gain.reshape(n0, n1, rows)
        twice = jnp.concatenate([blocks, blocks], axis=0)
        mine = lax.dynamic_slice_in_dim(twice, lax.axis_index("fs_0"), n0, 0)
        return jnp.stack([mine[o] for o in offsets], axis=1).reshape(-1)

    half = stream.shape[0] // 2
    stream = lax.dynamic_slice_in_dim(stream, core * half, half, 0)
    stream = dot(stream, chosen).astype(BF16)
    resid = stream.astype(F32)
    normed = norm_scale(resid, turned(mix_pre_gain)).astype(BF16)
    partial_value = 0.0
    for weights, taps in zip(mix_full, mix_taps):
        three = dot(normed, weights[:, : 3 * width]).astype(BF16).astype(F32)
        outer, inner, value = jnp.split(three, 3, axis=1)
        mixed = (outer * conv_three(inner * value, taps)).astype(BF16)
        partial_value = partial_value + dot_t(mixed, weights[:, 3 * width :])
    branch = rows_summed(partial_value)
    own_rows = branch.shape[0]
    own = lax.dynamic_slice_in_dim(stream, lax.axis_index("x") * own_rows, own_rows, 0)
    middle = own.astype(F32) + norm_scale(branch, turned(mix_post_gain))
    middle = middle.astype(BF16).astype(F32)
    normed_two = sent_to_all(norm_scale(middle, turned(ffn_pre_gain)).astype(BF16), "x")

    partial_two = 0.0
    for weights, extra in zip(ffn_full, small):
        both = dot(normed_two, weights[:, : 2 * hidden_w]).astype(BF16).astype(F32)
        linear, gated = both[:, :hidden_w], both[:, hidden_w:]
        activated = jax.nn.gelu(conv_three(gated, extra[:3]) + extra[3], approximate=True)
        hidden = (activated * linear).astype(BF16)
        partial_two = partial_two + dot_t(hidden, weights[:, 2 * hidden_w :])
    branch_two = rows_summed(partial_two)
    result = (middle + norm_scale(branch_two, turned(ffn_post_gain))).astype(BF16)
    result = sent_to_all(dot_t(result, chosen).astype(BF16), "x")
    return lax.all_gather(result, "core", axis=0, tiled=True)


def solution(mesh):
    split = Mesh(
        mesh.devices.reshape(mesh.shape["rep"], 8, 8, mesh.shape["tp"] // 2, 2),
        ("rep", "fs_0", "fs_1", "x", "core"),
    )
    return jax.shard_map(
        layer,
        mesh=split,
        in_specs=(
            P(REP_FS, None),
            P(),
            P(FS, TP),
            P(FS, TP),
            P(FS, TP),
            P(None, TP),
            P(TP, FS),
            P(),
            P(),
            P(FS, TP),
            P(FS, TP),
            P(None, TP),
            P(TP),
            P(TP, FS),
            P(),
        ),
        out_specs=P(REP_FS, None),
        check_vma=False,
    )
```

profile of v0, /device:TPU:1, one launch (start us, length us, event | category | flops | bytes accessed | tf_op | source)
XLA Modules:
  0.0 198.6 jit_solution(8268888144259353161)
XLA Ops:
  7.5 18.7 %collective-permute-start.5 = (bf16[24,1584]{1,0:T(8,128)(2,1)S(1)}, bf16[24,1584]{1,0:T(8,128)(2,1)S(1)}, u32[]{:S(2)}, u32[]{:S(2)}) collective-permute-start(bf16[24,1584]{1,0:T(8,128)(2,1)S(1)} %concatenate.48), channel_id=1, source_target_pairs={{0,768},{64,832},{128,896},{192,960},{256,0},{320,64},{384,128},{4... | collective-permute-start | bytes 228104 | tf_op jit(solution)/shard_map/ppermute | solution.py:18
  27.8 7.9 %collective-permute-start.6 = (bf16[48,1584]{1,0:T(8,128)(2,1)S(1)}, bf16[48,1584]{1,0:T(8,128)(2,1)S(1)}, u32[]{:S(2)}, u32[]{:S(2)}) collective-permute-start(bf16[48,1584]{1,0:T(8,128)(2,1)S(1)} %pad_maximum_fusion.4), channel_id=1, source_target_pairs={{0,896},{64,960},{128,0},{192,64},{256,128},{320,192},{384,256},{4... | collective-permute-start | bytes 456200 | tf_op jit(solution)/shard_map/ppermute | solution.py:18
  38.0 10.2 %collective-permute-start.7 = (bf16[96,1584]{1,0:T(8,128)(2,1)S(1)}, bf16[96,1584]{1,0:T(8,128)(2,1)S(1)}, u32[]{:S(2)}, u32[]{:S(2)}) collective-permute-start(bf16[96,1584]{1,0:T(8,128)(2,1)S(1)} %pad_maximum_fusion.2), channel_id=1, source_target_pairs={{0,960},{64,0},{128,64},{192,128},{256,192},{320,256},{384,320},{4... | collective-permute-start | bytes 912392 | tf_op jit(solution)/shard_map/ppermute | solution.py:18
  48.2 4.8 %collective-permute-done.7 = bf16[96,1584]{1,0:T(8,128)(2,1)S(1)} collective-permute-done((bf16[96,1584]{1,0:T(8,128)(2,1)S(1)}, bf16[96,1584]{1,0:T(8,128)(2,1)S(1)}, u32[]{:S(2)}, u32[]{:S(2)}) %collective-permute-start.7) | collective-permute-done | bytes 304160 | tf_op jit(solution)/shard_map/ppermute | solution.py:18
  54.6 3.4 %all-to-all-start = ((bf16[8,24,384]{2,1,0:T(8,128)(2,1)}), bf16[8,24,384]{2,1,0:T(8,128)(2,1)S(1)}, u32[]{:S(2)}, u32[]{:S(2)}) async-start(bf16[8,24,384]{2,1,0:T(8,128)(2,1)} %broadcast_in_dim.51), calls=%async_computation | async-start | bytes 294912 | tf_op jit(solution)/shard_map/all_to_all | solution.py:58
  58.1 6.2 %collective-permute-start.4 = (f32[7,528]{1,0:T(8,128)S(1)}, f32[7,528]{1,0:T(8,128)S(1)}, u32[]{:S(2)}, u32[]{:S(2)}) collective-permute-start(f32[7,528]{1,0:T(8,128)S(1)} %select_maximum_fusion), channel_id=1, source_target_pairs={{0,1},{1,0},{2,3},{3,2},{4,5},{5,4},{6,7},{7,6},{8,9},{9,8},{10,11... | collective-permute-start | bytes 44360 | tf_op jit(solution)/shard_map/ppermute | solution.py:33
  68.0 7.9 %collective-permute-done = bf16[192,384]{1,0:T(8,128)(2,1)S(1)} collective-permute-done((bf16[192,384]{1,0:T(8,128)(2,1)S(1)}, bf16[192,384]{1,0:T(8,128)(2,1)S(1)}, u32[]{:S(2)}, u32[]{:S(2)}) %collective-permute-start) | collective-permute-done | bytes 147488 | tf_op jit(solution)/shard_map/ppermute | solution.py:18
  80.1 9.1 %collective-permute-done.1 = bf16[384,384]{1,0:T(8,128)(2,1)S(1)} collective-permute-done((bf16[384,384]{1,0:T(8,128)(2,1)S(1)}, bf16[384,384]{1,0:T(8,128)(2,1)S(1)}, u32[]{:S(2)}, u32[]{:S(2)}) %collective-permute-start.1) | collective-permute-done | bytes 294944 | tf_op jit(solution)/shard_map/ppermute | solution.py:18
  89.3 6.0 %collective-permute-start.2 = (bf16[768,384]{1,0:T(8,128)(2,1)S(1)}, bf16[768,384]{1,0:T(8,128)(2,1)S(1)}, u32[]{:S(2)}, u32[]{:S(2)}) collective-permute-start(bf16[768,384]{1,0:T(8,128)(2,1)S(1)} %pad_maximum_fusion.1), channel_id=1, source_target_pairs={{0,64},{64,128},{128,192},{192,256},{256,320},{320,384},{384,448},... | collective-permute-start | bytes 1769480 | tf_op jit(solution)/shard_map/ppermute | solution.py:18
  95.5 12.6 %collective-permute-done.2 = bf16[768,384]{1,0:T(8,128)(2,1)S(1)} collective-permute-done((bf16[768,384]{1,0:T(8,128)(2,1)S(1)}, bf16[768,384]{1,0:T(8,128)(2,1)S(1)}, u32[]{:S(2)}, u32[]{:S(2)}) %collective-permute-start.2) | collective-permute-done | bytes 589856 | tf_op jit(solution)/shard_map/ppermute | solution.py:18
  108.3 11.7 %collective-permute-start.3 = (bf16[1536,384]{1,0:T(8,128)(2,1)S(1)}, bf16[1536,384]{1,0:T(8,128)(2,1)}, u32[]{:S(2)}, u32[]{:S(2)}) collective-permute-start(bf16[1536,384]{1,0:T(8,128)(2,1)S(1)} %bitcast.180), channel_id=1, source_target_pairs={{0,1},{1,0},{2,3},{3,2},{4,5},{5,4},{6,7},{7,6},{8,9},{9,8},{10,11... | collective-permute-start | bytes 3538952 | tf_op jit(solution)/shard_map/ppermute | solution.py:33
  124.7 2.3 %fusion.8 = bf16[128,1536]{1,0:T(8,128)(2,1)} fusion(f32[128,1536]{1,0:T(8,128)S(1)} %fusion.47, bf16[1536,384]{1,0:T(8,128)(2,1)} %collective-permute-done.3, f32[1,128,96]{1,2,0:T(8,128)S(1)} %fusion.144, f32[128,288]{0,1:T(8,128)S(1)} %fusion.40, f32[96]{0:T(128)S(1)} %get-tuple-element.56, f32[96]{0:T(128)S(1)} %get-tuple-element.57, ...), kind=kOutput, calls=%fused_computation.11 | convolution fusion | flops 38240256 | bytes 1770624 | tf_op jit(solution)/shard_map/dot_general | solution.py:53
  126.9 4.0 %all-to-all-start.1 = ((bf16[4,32,1536]{2,1,0:T(8,128)(2,1)}), bf16[4,32,1536]{2,1,0:T(8,128)(2,1)S(1)}, u32[]{:S(2)}, u32[]{:S(2)}) async-start(bf16[4,32,1536]{2,1,0:T(8,128)(2,1)} %bitcast.38), calls=%async_computation.1 | async-start | bytes 786432 | tf_op jit(solution)/shard_map/all_to_all | solution.py:65
  131.2 7.0 %all-to-all-done.1 = bf16[4,32,1536]{2,1,0:T(8,128)(2,1)S(1)} async-done(((bf16[4,32,1536]{2,1,0:T(8,128)(2,1)}), bf16[4,32,1536]{2,1,0:T(8,128)(2,1)S(1)}, u32[]{:S(2)}, u32[]{:S(2)}) %all-to-all-start.1) | async-done | bytes 393248 | tf_op jit(solution)/shard_map/all_to_all | solution.py:65
  139.5 3.6 %all-to-all-start.2 = ((bf16[4,32,1536]{2,1,0:T(8,128)(2,1)}), bf16[4,32,1536]{2,1,0:T(8,128)(2,1)S(1)}, u32[]{:S(2)}, u32[]{:S(2)}) async-start(bf16[4,32,1536]{2,1,0:T(8,128)(2,1)} %broadcast_in_dim.53), calls=%async_computation.2 | async-start | bytes 786432 | tf_op jit(solution)/shard_map/all_to_all | solution.py:58
  143.3 5.9 %all-to-all-done.2 = bf16[4,32,1536]{2,1,0:T(8,128)(2,1)S(1)} async-done(((bf16[4,32,1536]{2,1,0:T(8,128)(2,1)}), bf16[4,32,1536]{2,1,0:T(8,128)(2,1)S(1)}, u32[]{:S(2)}, u32[]{:S(2)}) %all-to-all-start.2) | async-done | bytes 393248 | tf_op jit(solution)/shard_map/all_to_all | solution.py:58
  149.2 3.5 %fusion.13 = f32[128,1056]{0,1:T(8,128)S(1)} fusion(bf16[128,1536]{1,0:T(8,128)(2,1)S(1)} %bitcast.178, bf16[3072,1584]{1,0:T(8,128)(2,1)} %all-gather.2.cloned.1.call-done), kind=kOutput, calls=%fused_computation.14 | convolution fusion | flops 415506432 | bytes 4472832 | tf_op jit(solution)/shard_map/dot_general | solution.py:49
  152.7 3.5 %fusion.19 = f32[128,1056]{0,1:T(8,128)S(1)} fusion(bf16[128,1536]{1,0:T(8,128)(2,1)S(1)} %bitcast.179, bf16[3072,1584]{1,0:T(8,128)(2,1)} %all-gather.2.cloned.1.call-done), kind=kOutput, calls=%fused_computation.16 | convolution fusion | flops 415506432 | bytes 4472832 | tf_op jit(solution)/shard_map/dot_general | solution.py:49
  156.2 3.1 %fusion.24 = f32[128,1536]{1,0:T(8,128)S(1)} fusion(bf16[3072,1584]{1,0:T(8,128)(2,1)} %all-gather.2.cloned.1.call-done, f32[1,128,528]{1,2,0:T(8,128)S(1)} %slice_bitcast_fusion, f32[128,1056]{0,1:T(8,128)S(1)} %fusion.19, f32[528]{0:T(1024)S(1)} %get-tuple-element.10, f32[528]{0:T(1024)S(1)} %get-tuple-element.11, f32[528]{0:T(1024)S(1)} %get-tuple-element.12, ...), kind=kOutput, calls=%fused_computation.19 | convolution fusion | flops 208699392 | bytes 3571968 | tf_op jit(solution)/shard_map/dot_general | solution.py:53
  159.3 3.9 %fusion.9 = bf16[128,1536]{1,0:T(8,128)(2,1)} fusion(f32[128,1536]{1,0:T(8,128)S(1)} %fusion.24, bf16[3072,1584]{1,0:T(8,128)(2,1)} %all-gather.2.cloned.1.call-done, f32[1,128,528]{1,2,0:T(8,128)S(1)} %slice_bitcast_fusion.1, f32[128,1056]{0,1:T(8,128)S(1)} %fusion.13, f32[528]{0:T(1024)S(1)} %get-tuple-element.69, f32[528]{0:T(1024)S(1)} %get-tuple-element.68, ...), kind=kOutput, calls=%fused_computation.12 | convolution fusion | flops 209092608 | bytes 3965184 | tf_op jit(solution)/shard_map/dot_general | solution.py:53
  163.2 3.5 %all-to-all-start.3 = ((bf16[4,32,1536]{2,1,0:T(8,128)(2,1)}), bf16[4,32,1536]{2,1,0:T(8,128)(2,1)S(1)}, u32[]{:S(2)}, u32[]{:S(2)}) async-start(bf16[4,32,1536]{2,1,0:T(8,128)(2,1)} %bitcast.77), calls=%async_computation.3 | async-start | bytes 786432 | tf_op jit(solution)/shard_map/all_to_all | solution.py:65
  166.9 6.0 %all-to-all-done.3 = bf16[4,32,1536]{2,1,0:T(8,128)(2,1)S(1)} async-done(((bf16[4,32,1536]{2,1,0:T(8,128)(2,1)}), bf16[4,32,1536]{2,1,0:T(8,128)(2,1)S(1)}, u32[]{:S(2)}, u32[]{:S(2)}) %all-to-all-start.3) | async-done | bytes 393248 | tf_op jit(solution)/shard_map/all_to_all | solution.py:65
  175.1 8.6 %all_to_all.25 = bf16[4,32,1536]{2,1,0:T(8,128)(2,1)S(1)} all-to-all(bf16[4,32,1536]{2,1,0:T(8,128)(2,1)S(1)} %broadcast_in_dim.54), channel_id=1, replica_groups=mesh['rep'=2,'fs_0'=8,'fs_1'=8,'x'=4,'core'=2] {'x'}, dimensions={0} | all-to-all | bytes 786432 | tf_op jit(solution)/shard_map/all_to_all | solution.py:58
  183.7 7.2 %all_gather.7 = bf16[256,1536]{1,0:T(8,128)(2,1)S(1)} all-gather(bf16[128,1536]{1,0:T(8,128)(2,1)S(1)} %bitcast.170), channel_id=1, replica_groups=mesh['rep'=2,'fs_0'=8,'fs_1'=8,'x'=4,'core'=2] {'core'}, dimensions={0}, use_global_device_ids=true | all-gather | bytes 1179648 | tf_op jit(solution)/shard_map/all_gather | solution.py:153
  (99 shorter events, 23.9 us)
Async XLA Ops:
  6.5 71.4 %copy-start = (bf16[256,1536]{1,0:T(8,128)(2,1)S(1)}, bf16[256,1536]{1,0:T(8,128)(2,1)}, u32[]{:S(2)}) copy-start(bf16[256,1536]{1,0:T(8,128)(2,1)} %param.15) | copy-start | bytes 2359300
  6.5 142.6 %all-gather.2.cloned.1.call-start = ((), (), s32[]{:S(2)}) async-start(), calls=%async_computation.5 | async-start | bytes 10862592 | tf_op jit(solution)/shard_map/all_gather | solution.py:95
  7.5 20.2 %collective-permute-start.5 = (bf16[24,1584]{1,0:T(8,128)(2,1)S(1)}, bf16[24,1584]{1,0:T(8,128)(2,1)S(1)}, u32[]{:S(2)}, u32[]{:S(2)}) collective-permute-start(bf16[24,1584]{1,0:T(8,128)(2,1)S(1)} %concatenate.48), channel_id=1, source_target_pairs={{0,768},{64,832},{128,896},{192,960},{256,0},{320,64},{384,128},{4... | collective-permute-start | bytes 228104 | tf_op jit(solution)/shard_map/ppermute | solution.py:18
  27.7 26.1 %copy-start.7 = (bf16[96,24]{0,1:T(8,128)(2,1)S(1)}, bf16[96,24]{0,1:T(8,128)(2,1)}, u32[]{:S(2)}) copy-start(bf16[96,24]{0,1:T(8,128)(2,1)} %param.21) | copy-start | bytes 13828
  27.7 26.1 %copy-start.8 = (bf16[24,96]{1,0:T(8,128)(2,1)S(1)}, bf16[24,96]{1,0:T(8,128)(2,1)}, u32[]{:S(2)}) copy-start(bf16[24,96]{1,0:T(8,128)(2,1)} %param.19) | copy-start | bytes 13828
  27.7 26.1 %copy-start.9 = (bf16[24,96]{1,0:T(8,128)(2,1)S(1)}, bf16[24,96]{1,0:T(8,128)(2,1)}, u32[]{:S(2)}) copy-start(bf16[24,96]{1,0:T(8,128)(2,1)} %param.18) | copy-start | bytes 13828
  27.7 26.1 %copy-start.10 = (bf16[24,96]{1,0:T(8,128)(2,1)S(1)}, bf16[24,96]{1,0:T(8,128)(2,1)}, u32[]{:S(2)}) copy-start(bf16[24,96]{1,0:T(8,128)(2,1)} %param.17) | copy-start | bytes 13828
  27.8 10.1 %collective-permute-start.6 = (bf16[48,1584]{1,0:T(8,128)(2,1)S(1)}, bf16[48,1584]{1,0:T(8,128)(2,1)S(1)}, u32[]{:S(2)}, u32[]{:S(2)}) collective-permute-start(bf16[48,1584]{1,0:T(8,128)(2,1)S(1)} %pad_maximum_fusion.4), channel_id=1, source_target_pairs={{0,896},{64,960},{128,0},{192,64},{256,128},{320,192},{384,256},{4... | collective-permute-start | bytes 456200 | tf_op jit(solution)/shard_map/ppermute | solution.py:18
  37.9 20.1 %copy-start.1 = (f32[3,528]{1,0:T(4,128)S(1)}, f32[3,528]{1,0:T(4,128)}, u32[]{:S(2)}) copy-start(f32[3,528]{1,0:T(4,128)} %param.26) | copy-start | bytes 19012
  37.9 20.1 %copy-start.2 = (f32[3,96]{1,0:T(4,128)S(1)}, f32[3,96]{1,0:T(4,128)}, u32[]{:S(2)}) copy-start(f32[3,96]{1,0:T(4,128)} %param.20) | copy-start | bytes 3460
  38.0 26.3 %copy-start.3 = (f32[1536]{0:T(1024)S(1)}, f32[1536]{0:T(1024)}, u32[]{:S(2)}) copy-start(f32[1536]{0:T(1024)} %param.16) | copy-start | bytes 18436
  38.0 26.4 %copy-start.4 = (f32[1536]{0:T(1024)S(1)}, f32[1536]{0:T(1024)}, u32[]{:S(2)}) copy-start(f32[1536]{0:T(1024)} %param.22) | copy-start | bytes 18436
  38.0 14.9 %collective-permute-start.7 = (bf16[96,1584]{1,0:T(8,128)(2,1)S(1)}, bf16[96,1584]{1,0:T(8,128)(2,1)S(1)}, u32[]{:S(2)}, u32[]{:S(2)}) collective-permute-start(bf16[96,1584]{1,0:T(8,128)(2,1)S(1)} %pad_maximum_fusion.2), channel_id=1, source_target_pairs={{0,960},{64,0},{128,64},{192,128},{256,192},{320,256},{384,320},{4... | collective-permute-start | bytes 912392 | tf_op jit(solution)/shard_map/ppermute | solution.py:18
  54.6 11.4 %all-to-all-start = ((bf16[8,24,384]{2,1,0:T(8,128)(2,1)}), bf16[8,24,384]{2,1,0:T(8,128)(2,1)S(1)}, u32[]{:S(2)}, u32[]{:S(2)}) async-start(bf16[8,24,384]{2,1,0:T(8,128)(2,1)} %broadcast_in_dim.51), calls=%async_computation | async-start | bytes 294912 | tf_op jit(solution)/shard_map/all_to_all | solution.py:58
  58.1 62.4 %collective-permute-start.4 = (f32[7,528]{1,0:T(8,128)S(1)}, f32[7,528]{1,0:T(8,128)S(1)}, u32[]{:S(2)}, u32[]{:S(2)}) collective-permute-start(f32[7,528]{1,0:T(8,128)S(1)} %select_maximum_fusion), channel_id=1, source_target_pairs={{0,1},{1,0},{2,3},{3,2},{4,5},{5,4},{6,7},{7,6},{8,9},{9,8},{10,11... | collective-permute-start | bytes 44360 | tf_op jit(solution)/shard_map/ppermute | solution.py:33
  66.0 9.9 %collective-permute-start = (bf16[192,384]{1,0:T(8,128)(2,1)S(1)}, bf16[192,384]{1,0:T(8,128)(2,1)S(1)}, u32[]{:S(2)}, u32[]{:S(2)}) collective-permute-start(bf16[192,384]{1,0:T(8,128)(2,1)S(1)} %bitcast.167), channel_id=1, source_target_pairs={{0,256},{64,320},{128,384},{192,448},{256,512},{320,576},{384,640}... | collective-permute-start | bytes 442376 | tf_op jit(solution)/shard_map/ppermute | solution.py:18
  75.9 13.3 %collective-permute-start.1 = (bf16[384,384]{1,0:T(8,128)(2,1)S(1)}, bf16[384,384]{1,0:T(8,128)(2,1)S(1)}, u32[]{:S(2)}, u32[]{:S(2)}) collective-permute-start(bf16[384,384]{1,0:T(8,128)(2,1)S(1)} %pad_maximum_fusion.3), channel_id=1, source_target_pairs={{0,128},{64,192},{128,256},{192,320},{256,384},{320,448},{384,512}... | collective-permute-start | bytes 884744 | tf_op jit(solution)/shard_map/ppermute | solution.py:18
  89.3 18.8 %collective-permute-start.2 = (bf16[768,384]{1,0:T(8,128)(2,1)S(1)}, bf16[768,384]{1,0:T(8,128)(2,1)S(1)}, u32[]{:S(2)}, u32[]{:S(2)}) collective-permute-start(bf16[768,384]{1,0:T(8,128)(2,1)S(1)} %pad_maximum_fusion.1), channel_id=1, source_target_pairs={{0,64},{64,128},{128,192},{192,256},{256,320},{320,384},{384,448},... | collective-permute-start | bytes 1769480 | tf_op jit(solution)/shard_map/ppermute | solution.py:18
  95.4 24.9 %copy-start.5 = (f32[1536]{0:T(1024)S(1)}, f32[1536]{0:T(1024)}, u32[]{:S(2)}) copy-start(f32[1536]{0:T(1024)} %param.23) | copy-start | bytes 18436
  95.5 25.0 %copy-start.6 = (f32[1536]{0:T(1024)S(1)}, f32[1536]{0:T(1024)}, u32[]{:S(2)}) copy-start(f32[1536]{0:T(1024)} %param.29) | copy-start | bytes 18436
  108.3 14.5 %collective-permute-start.3 = (bf16[1536,384]{1,0:T(8,128)(2,1)S(1)}, bf16[1536,384]{1,0:T(8,128)(2,1)}, u32[]{:S(2)}, u32[]{:S(2)}) collective-permute-start(bf16[1536,384]{1,0:T(8,128)(2,1)S(1)} %bitcast.180), channel_id=1, source_target_pairs={{0,1},{1,0},{2,3},{3,2},{4,5},{5,4},{6,7},{7,6},{8,9},{9,8},{10,11... | collective-permute-start | bytes 3538952 | tf_op jit(solution)/shard_map/ppermute | solution.py:33
  126.9 11.3 %all-to-all-start.1 = ((bf16[4,32,1536]{2,1,0:T(8,128)(2,1)}), bf16[4,32,1536]{2,1,0:T(8,128)(2,1)S(1)}, u32[]{:S(2)}, u32[]{:S(2)}) async-start(bf16[4,32,1536]{2,1,0:T(8,128)(2,1)} %bitcast.38), calls=%async_computation.1 | async-start | bytes 786432 | tf_op jit(solution)/shard_map/all_to_all | solution.py:65
  139.5 9.7 %all-to-all-start.2 = ((bf16[4,32,1536]{2,1,0:T(8,128)(2,1)}), bf16[4,32,1536]{2,1,0:T(8,128)(2,1)S(1)}, u32[]{:S(2)}, u32[]{:S(2)}) async-start(bf16[4,32,1536]{2,1,0:T(8,128)(2,1)} %broadcast_in_dim.53), calls=%async_computation.2 | async-start | bytes 786432 | tf_op jit(solution)/shard_map/all_to_all | solution.py:58
  163.2 9.7 %all-to-all-start.3 = ((bf16[4,32,1536]{2,1,0:T(8,128)(2,1)}), bf16[4,32,1536]{2,1,0:T(8,128)(2,1)S(1)}, u32[]{:S(2)}, u32[]{:S(2)}) async-start(bf16[4,32,1536]{2,1,0:T(8,128)(2,1)} %bitcast.77), calls=%async_computation.3 | async-start | bytes 786432 | tf_op jit(solution)/shard_map/all_to_all | solution.py:65
  (1 other events, 20.1 us)
Sparse Core Ops, SparseCore 0:
  54.0 69.9 all-gather.1
where the time goes:
time: 200 us; the launch traced here: 199 us
  starting transfers between devices  79.1 us (40%)
  waiting for transfers between devices  59.7 us (30%)
  matrix products  23.3 us (12%)
  blocking collectives  15.9 us (8%)
  between operations  14 us (7%)
  local copies, waits for them, and re-layouts  4.73 us (2%)
    ppermute x6, starting transfers between devices, from_ahead(): lax.ppermute(x, ('rep', 'fs_0'), [(i, (i - steps) % n) for i in range(n)])  46.6 us
    ppermute x6, waiting for transfers between devices, from_ahead(): lax.ppermute(x, ('rep', 'fs_0'), [(i, (i - steps) % n) for i in range(n)])  38.1 us
    ppermute x2, starting transfers between devices, other_core(): return lax.ppermute(x, 'core', [(0, 1), (1, 0)])  17.9 us
    all_to_all x2, waiting for transfers between devices, rows_summed(): lax.all_to_all(tiles, 'x', split_axis=0, concat_axis=0, tiled=True)  13.1 us
    dot_general x5, matrix products, dot_t(): lax.dot_general(a, b, (((1,), (1,)), ((), ())), preferred_element_type=F32)  11.8 us
    dot_general x5, matrix products, dot(): return jnp.dot(a, b, preferred_element_type=F32)  11.5 us
    all_to_all x1, blocking collectives, sent_to_all(): lax.all_to_all(jnp.broadcast_to(x[None], (n, *x.shape)), axis, 0, 0, tile...  8.62 us
    all_to_all x2, starting transfers between devices, rows_summed(): lax.all_to_all(tiles, 'x', split_axis=0, concat_axis=0, tiled=True)  7.5 us
  transfers between devices with their start and end apart: 13, of which 11 were waited for; matrix products, arithmetic and copies ran while one was open for 6% of the time, Pallas kernels for 0%

commit v1 on v0

--- a/solution.py
+++ b/solution.py
@@ -18,15 +18,12 @@
     return lax.ppermute(x, ("rep", "fs_0"), [(i, (i - steps) % n) for i in range(n)])
 
 
-def doubled(x, sign):
-    n = lax.axis_size("fs_0")
-    offsets, step = [0], n // 2
-    while step:
+def doubled(x, offsets, steps, sign):
+    for step in steps:
         arrived = from_ahead(x, sign * step)
         x = jnp.concatenate([x, arrived], axis=0)
-        offsets += [o + sign * step for o in offsets]
-        step //= 2
-    return x, [o % n for o in offsets]
+        offsets = offsets + [o + sign * step for o in offsets]
+    return x, [o % lax.axis_size("fs_0") for o in offsets]
 
 
 def other_core(x):
@@ -91,15 +88,21 @@
     core = lax.axis_index("core")
 
     ffn_cols = jnp.concatenate([w_linear, w_gated, w_down.T], axis=1)
-    ffn_part, offsets = doubled(ffn_cols, 1)
+    ffn_part, offsets = doubled(ffn_cols, [0], (4, 2, 1), 1)
     ffn_full = lax.all_gather(ffn_part, ("core", "fs_1"), axis=0, tiled=True)
     ffn_full = [ffn_full[:d], ffn_full[d:]]
 
     mix_cols = jnp.concatenate([w_outer_gate, w_inner_gate, w_value, w_mix_out.T], axis=1)
     mix_part = sent_to_all(mix_cols, "fs_1")
-    mix_part, back = doubled(mix_part, -1)
-    mix_part = mix_part.reshape(n0, n1, rows, mix_cols.shape[1])
-    mix_own = jnp.stack([mix_part[back.index(o)] for o in offsets], axis=1).reshape(d, -1)
+    mix_part, near = doubled(mix_part, [0], (4,), -1)
+    mix_part = mix_part.reshape(len(near), 2, -1, mix_part.shape[1])
+    ways = []
+    for way, sign in ((0, -1), (1, 1)):
+        mine = mix_part[:, way].reshape(-1, mix_part.shape[3])
+        mine, back = doubled(mine, near, (2, 1), sign)
+        mine = mine.reshape(n0, n1 // 2, rows, -1)
+        ways.append(jnp.stack([mine[back.index(o)] for o in offsets], axis=1))
+    mix_own = jnp.concatenate(ways, axis=0).reshape(d, -1)
     mix_full = [mix_own, other_core(mix_own)]
 
     small = jnp.concatenate(

time: 200 us -> 195 us (0.975)
  waiting for transfers between devices: 59.7 us -> 41.7 us
  starting transfers between devices: 79.1 us -> 92.2 us
    ppermute x6 -> x8, starting transfers between devices: 46.6 us -> 67.2 us  [from_ahead(): lax.ppermute(x, ('rep', 'fs_0'), [(i, (i - steps) % n) for i in range(n)])]
    ppermute x6 -> x8, waiting for transfers between devices: 38.1 us -> 22.6 us  [from_ahead(): lax.ppermute(x, ('rep', 'fs_0'), [(i, (i - steps) % n) for i in range(n)])]
    ppermute x2, starting transfers between devices: 17.9 us -> 10.5 us  [other_core(): return lax.ppermute(x, 'core', [(0, 1), (1, 0)])]
  transfers between devices with their start and end apart: 13 -> 15, of which waited for: 11 -> 9; matrix products, arithmetic and copies ran while one was open for 6% -> 6% of each run, Pallas kernels for 0% -> 0%
where the time goes in v1:
time: 195 us; the launch traced here: 194 us
  starting transfers between devices  92.2 us (47%)
  waiting for transfers between devices  41.7 us (21%)
  matrix products  22.8 us (12%)
  blocking collectives  15.8 us (8%)
  between operations  14.1 us (7%)
  local copies, waits for them, and re-layouts  4.87 us (2%)
  other arithmetic  3.02 us (2%)
    ppermute x8, starting transfers between devices, from_ahead(): lax.ppermute(x, ('rep', 'fs_0'), [(i, (i - steps) % n) for i in range(n)])  67.2 us
    ppermute x8, waiting for transfers between devices, from_ahead(): lax.ppermute(x, ('rep', 'fs_0'), [(i, (i - steps) % n) for i in range(n)])  22.6 us
    all_to_all x2, waiting for transfers between devices, rows_summed(): lax.all_to_all(tiles, 'x', split_axis=0, concat_axis=0, tiled=True)  13.1 us
    dot_general x5, matrix products, dot(): return jnp.dot(a, b, preferred_element_type=F32)  12 us
    dot_general x5, matrix products, dot_t(): lax.dot_general(a, b, (((1,), (1,)), ((), ())), preferred_element_type=F32)  10.8 us
    ppermute x2, starting transfers between devices, other_core(): return lax.ppermute(x, 'core', [(0, 1), (1, 0)])  10.5 us
    all_to_all x1, blocking collectives, sent_to_all(): lax.all_to_all(jnp.broadcast_to(x[None], (n, *x.shape)), axis, 0, 0, tile...  8.62 us
    all_to_all x2, starting transfers between devices, rows_summed(): lax.all_to_all(tiles, 'x', split_axis=0, concat_axis=0, tiled=True)  7.53 us
  transfers between devices with their start and end apart: 15, of which 9 were waited for; matrix products, arithmetic and copies ran while one was open for 6% of the time, Pallas kernels for 0%

profile of v1, /device:TPU:1, one launch (start us, length us, event | category | flops | bytes accessed | tf_op | source)
XLA Modules:
  0.0 194.4 jit_solution(13176623367321232401)
XLA Ops:
  7.6 18.7 %collective-permute-start.7 = (bf16[24,1584]{1,0:T(8,128)(2,1)S(1)}, bf16[24,1584]{1,0:T(8,128)(2,1)S(1)}, u32[]{:S(2)}, u32[]{:S(2)}) collective-permute-start(bf16[24,1584]{1,0:T(8,128)(2,1)S(1)} %concatenate.57), channel_id=1, source_target_pairs={{0,768},{64,832},{128,896},{192,960},{256,0},{320,64},{384,128},{4... | collective-permute-start | bytes 228104 | tf_op jit(solution)/shard_map/ppermute | solution.py:18
  27.8 7.8 %collective-permute-start.8 = (bf16[48,1584]{1,0:T(8,128)(2,1)S(1)}, bf16[48,1584]{1,0:T(8,128)(2,1)S(1)}, u32[]{:S(2)}, u32[]{:S(2)}) collective-permute-start(bf16[48,1584]{1,0:T(8,128)(2,1)S(1)} %pad_maximum_fusion.6), channel_id=1, source_target_pairs={{0,896},{64,960},{128,0},{192,64},{256,128},{320,192},{384,256},{4... | collective-permute-start | bytes 456200 | tf_op jit(solution)/shard_map/ppermute | solution.py:18
  37.9 10.1 %collective-permute-start.9 = (bf16[96,1584]{1,0:T(8,128)(2,1)S(1)}, bf16[96,1584]{1,0:T(8,128)(2,1)S(1)}, u32[]{:S(2)}, u32[]{:S(2)}) collective-permute-start(bf16[96,1584]{1,0:T(8,128)(2,1)S(1)} %pad_maximum_fusion.2), channel_id=1, source_target_pairs={{0,960},{64,0},{128,64},{192,128},{256,192},{320,256},{384,320},{4... | collective-permute-start | bytes 912392 | tf_op jit(solution)/shard_map/ppermute | solution.py:18
  47.9 4.9 %collective-permute-done.9 = bf16[96,1584]{1,0:T(8,128)(2,1)S(1)} collective-permute-done((bf16[96,1584]{1,0:T(8,128)(2,1)S(1)}, bf16[96,1584]{1,0:T(8,128)(2,1)S(1)}, u32[]{:S(2)}, u32[]{:S(2)}) %collective-permute-start.9) | collective-permute-done | bytes 304160 | tf_op jit(solution)/shard_map/ppermute | solution.py:18
  54.5 3.4 %all-to-all-start = ((bf16[8,24,384]{2,1,0:T(8,128)(2,1)}), bf16[8,24,384]{2,1,0:T(8,128)(2,1)S(1)}, u32[]{:S(2)}, u32[]{:S(2)}) async-start(bf16[8,24,384]{2,1,0:T(8,128)(2,1)} %broadcast_in_dim.51), calls=%async_computation | async-start | bytes 294912 | tf_op jit(solution)/shard_map/all_to_all | solution.py:55
  58.0 6.1 %collective-permute-start.6 = (f32[7,528]{1,0:T(8,128)S(1)}, f32[7,528]{1,0:T(8,128)S(1)}, u32[]{:S(2)}, u32[]{:S(2)}) collective-permute-start(f32[7,528]{1,0:T(8,128)S(1)} %select_maximum_fusion), channel_id=1, source_target_pairs={{0,1},{1,0},{2,3},{3,2},{4,5},{5,4},{6,7},{7,6},{8,9},{9,8},{10,11... | collective-permute-start | bytes 44360 | tf_op jit(solution)/shard_map/ppermute | solution.py:30
  64.4 2.9 %fusion.43 = (f32[128]{0:T(128)S(1)}, bf16[128,1536]{1,0:T(8,128)(2,1)}) fusion(s32[1536]{0:T(1024)S(1)} %fusion.149, bf16[256,1536]{1,0:T(8,128)(2,1)S(1)} %copy-done, s32[]{:T(128)S(6)} %select_n.118), kind=kOutput, calls=%fused_computation.33 | convolution fusion | flops 607125376 | bytes 795140 | tf_op jit(solution)/shard_map/dot_general | solution.py:46
  70.1 7.0 %collective-permute-done = bf16[192,384]{1,0:T(8,128)(2,1)S(1)} collective-permute-done((bf16[192,384]{1,0:T(8,128)(2,1)S(1)}, bf16[192,384]{1,0:T(8,128)(2,1)S(1)}, u32[]{:S(2)}, u32[]{:S(2)}) %collective-permute-start) | collective-permute-done | bytes 147488 | tf_op jit(solution)/shard_map/ppermute | solution.py:18
  77.2 9.2 %collective-permute-start.3 = (bf16[192,384]{1,0:T(8,128)(2,1)S(1)}, bf16[192,384]{1,0:T(8,128)(2,1)S(1)}, u32[]{:S(2)}, u32[]{:S(2)}) collective-permute-start(bf16[192,384]{1,0:T(8,128)(2,1)S(1)} %bitcast.187), channel_id=1, source_target_pairs={{0,896},{64,960},{128,0},{192,64},{256,128},{320,192},{384,256},{4... | collective-permute-start | bytes 442376 | tf_op jit(solution)/shard_map/ppermute | solution.py:18
  88.5 13.8 %collective-permute-start.4 = (bf16[384,384]{1,0:T(8,128)(2,1)S(1)}, bf16[384,384]{1,0:T(8,128)(2,1)S(1)}, u32[]{:S(2)}, u32[]{:S(2)}) collective-permute-start(bf16[384,384]{1,0:T(8,128)(2,1)S(1)} %pad_maximum_fusion.5), channel_id=1, source_target_pairs={{0,960},{64,0},{128,64},{192,128},{256,192},{320,256},{384,320},{4... | collective-permute-start | bytes 884744 | tf_op jit(solution)/shard_map/ppermute | solution.py:18
  107.4 5.1 %collective-permute-done.2 = bf16[384,384]{1,0:T(8,128)(2,1)S(1)} collective-permute-done((bf16[384,384]{1,0:T(8,128)(2,1)S(1)}, bf16[384,384]{1,0:T(8,128)(2,1)S(1)}, u32[]{:S(2)}, u32[]{:S(2)}) %collective-permute-start.2) | collective-permute-done | bytes 294944 | tf_op jit(solution)/shard_map/ppermute | solution.py:18
  112.7 4.4 %collective-permute-start.5 = (bf16[1536,384]{1,0:T(8,128)(2,1)S(1)}, bf16[1536,384]{1,0:T(8,128)(2,1)S(1)}, u32[]{:S(2)}, u32[]{:S(2)}) collective-permute-start(bf16[1536,384]{1,0:T(8,128)(2,1)S(1)} %bitcast.179), channel_id=1, source_target_pairs={{0,1},{1,0},{2,3},{3,2},{4,5},{5,4},{6,7},{7,6},{8,9},{9,8},{10,11... | collective-permute-start | bytes 3538952 | tf_op jit(solution)/shard_map/ppermute | solution.py:30
  121.7 4.1 %all-to-all-start.1 = ((bf16[4,32,1536]{2,1,0:T(8,128)(2,1)}), bf16[4,32,1536]{2,1,0:T(8,128)(2,1)S(1)}, u32[]{:S(2)}, u32[]{:S(2)}) async-start(bf16[4,32,1536]{2,1,0:T(8,128)(2,1)} %bitcast.49), calls=%async_computation.1 | async-start | bytes 786432 | tf_op jit(solution)/shard_map/all_to_all | solution.py:62
  126.0 7.1 %all-to-all-done.1 = bf16[4,32,1536]{2,1,0:T(8,128)(2,1)S(1)} async-done(((bf16[4,32,1536]{2,1,0:T(8,128)(2,1)}), bf16[4,32,1536]{2,1,0:T(8,128)(2,1)S(1)}, u32[]{:S(2)}, u32[]{:S(2)}) %all-to-all-start.1) | async-done | bytes 393248 | tf_op jit(solution)/shard_map/all_to_all | solution.py:62
  135.3 3.6 %all-to-all-start.2 = ((bf16[4,32,1536]{2,1,0:T(8,128)(2,1)}), bf16[4,32,1536]{2,1,0:T(8,128)(2,1)S(1)}, u32[]{:S(2)}, u32[]{:S(2)}) async-start(bf16[4,32,1536]{2,1,0:T(8,128)(2,1)} %broadcast_in_dim.53), calls=%async_computation.2 | async-start | bytes 786432 | tf_op jit(solution)/shard_map/all_to_all | solution.py:55
  139.1 5.9 %all-to-all-done.2 = bf16[4,32,1536]{2,1,0:T(8,128)(2,1)S(1)} async-done(((bf16[4,32,1536]{2,1,0:T(8,128)(2,1)}), bf16[4,32,1536]{2,1,0:T(8,128)(2,1)S(1)}, u32[]{:S(2)}, u32[]{:S(2)}) %all-to-all-start.2) | async-done | bytes 393248 | tf_op jit(solution)/shard_map/all_to_all | solution.py:55
  145.0 3.5 %fusion.13 = f32[128,1056]{0,1:T(8,128)S(1)} fusion(bf16[128,1536]{1,0:T(8,128)(2,1)S(1)} %bitcast.189, bf16[3072,1584]{1,0:T(8,128)(2,1)} %all-gather.2.cloned.1.call-done), kind=kOutput, calls=%fused_computation.14 | convolution fusion | flops 415506432 | bytes 4472832 | tf_op jit(solution)/shard_map/dot_general | solution.py:46
  148.5 3.5 %fusion.19 = f32[128,1056]{0,1:T(8,128)S(1)} fusion(bf16[128,1536]{1,0:T(8,128)(2,1)S(1)} %bitcast.190, bf16[3072,1584]{1,0:T(8,128)(2,1)} %all-gather.2.cloned.1.call-done), kind=kOutput, calls=%fused_computation.16 | convolution fusion | flops 415506432 | bytes 4472832 | tf_op jit(solution)/shard_map/dot_general | solution.py:46
  152.0 3.1 %fusion.24 = f32[128,1536]{1,0:T(8,128)S(1)} fusion(bf16[3072,1584]{1,0:T(8,128)(2,1)} %all-gather.2.cloned.1.call-done, f32[1,128,528]{1,2,0:T(8,128)S(1)} %slice_bitcast_fusion, f32[128,1056]{0,1:T(8,128)S(1)} %fusion.19, f32[528]{0:T(1024)S(1)} %get-tuple-element.10, f32[528]{0:T(1024)S(1)} %get-tuple-element.11, f32[528]{0:T(1024)S(1)} %get-tuple-element.12, ...), kind=kOutput, calls=%fused_computation.19 | convolution fusion | flops 208699392 | bytes 3571968 | tf_op jit(solution)/shard_map/dot_general | solution.py:50
  155.1 3.9 %fusion.9 = bf16[128,1536]{1,0:T(8,128)(2,1)} fusion(f32[128,1536]{1,0:T(8,128)S(1)} %fusion.24, bf16[3072,1584]{1,0:T(8,128)(2,1)} %all-gather.2.cloned.1.call-done, f32[1,128,528]{1,2,0:T(8,128)S(1)} %slice_bitcast_fusion.1, f32[128,1056]{0,1:T(8,128)S(1)} %fusion.13, f32[528]{0:T(1024)S(1)} %get-tuple-element.83, f32[528]{0:T(1024)S(1)} %get-tuple-element.82, ...), kind=kOutput, calls=%fused_computation.12 | convolution fusion | flops 209092608 | bytes 3965184 | tf_op jit(solution)/shard_map/dot_general | solution.py:50
  159.0 3.5 %all-to-all-start.3 = ((bf16[4,32,1536]{2,1,0:T(8,128)(2,1)}), bf16[4,32,1536]{2,1,0:T(8,128)(2,1)S(1)}, u32[]{:S(2)}, u32[]{:S(2)}) async-start(bf16[4,32,1536]{2,1,0:T(8,128)(2,1)} %bitcast.88), calls=%async_computation.3 | async-start | bytes 786432 | tf_op jit(solution)/shard_map/all_to_all | solution.py:62
  162.7 6.0 %all-to-all-done.3 = bf16[4,32,1536]{2,1,0:T(8,128)(2,1)S(1)} async-done(((bf16[4,32,1536]{2,1,0:T(8,128)(2,1)}), bf16[4,32,1536]{2,1,0:T(8,128)(2,1)S(1)}, u32[]{:S(2)}, u32[]{:S(2)}) %all-to-all-start.3) | async-done | bytes 393248 | tf_op jit(solution)/shard_map/all_to_all | solution.py:62
  170.9 8.6 %all_to_all.25 = bf16[4,32,1536]{2,1,0:T(8,128)(2,1)S(1)} all-to-all(bf16[4,32,1536]{2,1,0:T(8,128)(2,1)S(1)} %broadcast_in_dim.54), channel_id=1, replica_groups=mesh['rep'=2,'fs_0'=8,'fs_1'=8,'x'=4,'core'=2] {'x'}, dimensions={0} | all-to-all | bytes 786432 | tf_op jit(solution)/shard_map/all_to_all | solution.py:55
  179.5 7.2 %all_gather.7 = bf16[256,1536]{1,0:T(8,128)(2,1)S(1)} all-gather(bf16[128,1536]{1,0:T(8,128)(2,1)S(1)} %bitcast.182), channel_id=1, replica_groups=mesh['rep'=2,'fs_0'=8,'fs_1'=8,'x'=4,'core'=2] {'core'}, dimensions={0}, use_global_device_ids=true | all-gather | bytes 1179648 | tf_op jit(solution)/shard_map/all_gather | solution.py:156
  (118 shorter events, 27.0 us)
Async XLA Ops:
  6.5 57.8 %copy-start = (bf16[256,1536]{1,0:T(8,128)(2,1)S(1)}, bf16[256,1536]{1,0:T(8,128)(2,1)}, u32[]{:S(2)}) copy-start(bf16[256,1536]{1,0:T(8,128)(2,1)} %param.15) | copy-start | bytes 2359300
  6.5 47.2 %copy-start.11 = (bf16[24,96]{1,0:T(8,128)(2,1)S(1)}, bf16[24,96]{1,0:T(8,128)(2,1)}, u32[]{:S(2)}) copy-start(bf16[24,96]{1,0:T(8,128)(2,1)} %param.17) | copy-start | bytes 13828
  6.5 47.2 %copy-start.10 = (bf16[24,96]{1,0:T(8,128)(2,1)S(1)}, bf16[24,96]{1,0:T(8,128)(2,1)}, u32[]{:S(2)}) copy-start(bf16[24,96]{1,0:T(8,128)(2,1)} %param.18) | copy-start | bytes 13828
  6.5 47.2 %copy-start.9 = (bf16[24,96]{1,0:T(8,128)(2,1)S(1)}, bf16[24,96]{1,0:T(8,128)(2,1)}, u32[]{:S(2)}) copy-start(bf16[24,96]{1,0:T(8,128)(2,1)} %param.19) | copy-start | bytes 13828
  6.5 51.4 %copy-start.12 = (f32[528]{0:T(1024)S(1)}, f32[528]{0:T(1024)}, u32[]{:S(2)}) copy-start(f32[528]{0:T(1024)} %param.27) | copy-start | bytes 6340
  6.6 51.4 %copy-start.3 = (f32[3,96]{1,0:T(4,128)S(1)}, f32[3,96]{1,0:T(4,128)}, u32[]{:S(2)}) copy-start(f32[3,96]{1,0:T(4,128)} %param.20) | copy-start | bytes 3460
  6.6 51.4 %copy-start.1 = (f32[3,528]{1,0:T(4,128)S(1)}, f32[3,528]{1,0:T(4,128)}, u32[]{:S(2)}) copy-start(f32[3,528]{1,0:T(4,128)} %param.26) | copy-start | bytes 19012
  6.6 57.5 %copy-start.4 = (f32[1536]{0:T(1024)S(1)}, f32[1536]{0:T(1024)}, u32[]{:S(2)}) copy-start(f32[1536]{0:T(1024)} %param.16) | copy-start | bytes 18436
  6.6 57.5 %copy-start.5 = (f32[1536]{0:T(1024)S(1)}, f32[1536]{0:T(1024)}, u32[]{:S(2)}) copy-start(f32[1536]{0:T(1024)} %param.22) | copy-start | bytes 18436
  6.6 138.4 %all-gather.2.cloned.1.call-start = ((), (), s32[]{:S(2)}) async-start(), calls=%async_computation.5 | async-start | bytes 10862592 | tf_op jit(solution)/shard_map/all_gather | solution.py:92
  7.6 20.2 %collective-permute-start.7 = (bf16[24,1584]{1,0:T(8,128)(2,1)S(1)}, bf16[24,1584]{1,0:T(8,128)(2,1)S(1)}, u32[]{:S(2)}, u32[]{:S(2)}) collective-permute-start(bf16[24,1584]{1,0:T(8,128)(2,1)S(1)} %concatenate.57), channel_id=1, source_target_pairs={{0,768},{64,832},{128,896},{192,960},{256,0},{320,64},{384,128},{4... | collective-permute-start | bytes 228104 | tf_op jit(solution)/shard_map/ppermute | solution.py:18
  27.8 10.0 %collective-permute-start.8 = (bf16[48,1584]{1,0:T(8,128)(2,1)S(1)}, bf16[48,1584]{1,0:T(8,128)(2,1)S(1)}, u32[]{:S(2)}, u32[]{:S(2)}) collective-permute-start(bf16[48,1584]{1,0:T(8,128)(2,1)S(1)} %pad_maximum_fusion.6), channel_id=1, source_target_pairs={{0,896},{64,960},{128,0},{192,64},{256,128},{320,192},{384,256},{4... | collective-permute-start | bytes 456200 | tf_op jit(solution)/shard_map/ppermute | solution.py:18
  37.9 15.0 %collective-permute-start.9 = (bf16[96,1584]{1,0:T(8,128)(2,1)S(1)}, bf16[96,1584]{1,0:T(8,128)(2,1)S(1)}, u32[]{:S(2)}, u32[]{:S(2)}) collective-permute-start(bf16[96,1584]{1,0:T(8,128)(2,1)S(1)} %pad_maximum_fusion.2), channel_id=1, source_target_pairs={{0,960},{64,0},{128,64},{192,128},{256,192},{320,256},{384,320},{4... | collective-permute-start | bytes 912392 | tf_op jit(solution)/shard_map/ppermute | solution.py:18
  54.5 12.7 %all-to-all-start = ((bf16[8,24,384]{2,1,0:T(8,128)(2,1)}), bf16[8,24,384]{2,1,0:T(8,128)(2,1)S(1)}, u32[]{:S(2)}, u32[]{:S(2)}) async-start(bf16[8,24,384]{2,1,0:T(8,128)(2,1)} %broadcast_in_dim.51), calls=%async_computation | async-start | bytes 294912 | tf_op jit(solution)/shard_map/all_to_all | solution.py:55
  58.0 59.7 %collective-permute-start.6 = (f32[7,528]{1,0:T(8,128)S(1)}, f32[7,528]{1,0:T(8,128)S(1)}, u32[]{:S(2)}, u32[]{:S(2)}) collective-permute-start(f32[7,528]{1,0:T(8,128)S(1)} %select_maximum_fusion), channel_id=1, source_target_pairs={{0,1},{1,0},{2,3},{3,2},{4,5},{5,4},{6,7},{7,6},{8,9},{9,8},{10,11... | collective-permute-start | bytes 44360 | tf_op jit(solution)/shard_map/ppermute | solution.py:30
  67.2 9.9 %collective-permute-start = (bf16[192,384]{1,0:T(8,128)(2,1)S(1)}, bf16[192,384]{1,0:T(8,128)(2,1)S(1)}, u32[]{:S(2)}, u32[]{:S(2)}) collective-permute-start(bf16[192,384]{1,0:T(8,128)(2,1)S(1)} %bitcast.183), channel_id=1, source_target_pairs={{0,256},{64,320},{128,384},{192,448},{256,512},{320,576},{384,640}... | collective-permute-start | bytes 442376 | tf_op jit(solution)/shard_map/ppermute | solution.py:18
  77.2 11.3 %collective-permute-start.3 = (bf16[192,384]{1,0:T(8,128)(2,1)S(1)}, bf16[192,384]{1,0:T(8,128)(2,1)S(1)}, u32[]{:S(2)}, u32[]{:S(2)}) collective-permute-start(bf16[192,384]{1,0:T(8,128)(2,1)S(1)} %bitcast.187), channel_id=1, source_target_pairs={{0,896},{64,960},{128,0},{192,64},{256,128},{320,192},{384,256},{4... | collective-permute-start | bytes 442376 | tf_op jit(solution)/shard_map/ppermute | solution.py:18
  86.4 15.9 %collective-permute-start.1 = (bf16[192,384]{1,0:T(8,128)(2,1)S(1)}, bf16[192,384]{1,0:T(8,128)(2,1)S(1)}, u32[]{:S(2)}, u32[]{:S(2)}) collective-permute-start(bf16[192,384]{1,0:T(8,128)(2,1)S(1)} %bitcast.185), channel_id=1, source_target_pairs={{0,128},{64,192},{128,256},{192,320},{256,384},{320,448},{384,512}... | collective-permute-start | bytes 442376 | tf_op jit(solution)/shard_map/ppermute | solution.py:18
  88.5 18.7 %collective-permute-start.4 = (bf16[384,384]{1,0:T(8,128)(2,1)S(1)}, bf16[384,384]{1,0:T(8,128)(2,1)S(1)}, u32[]{:S(2)}, u32[]{:S(2)}) collective-permute-start(bf16[384,384]{1,0:T(8,128)(2,1)S(1)} %pad_maximum_fusion.5), channel_id=1, source_target_pairs={{0,960},{64,0},{128,64},{192,128},{256,192},{320,256},{384,320},{4... | collective-permute-start | bytes 884744 | tf_op jit(solution)/shard_map/ppermute | solution.py:18
  102.4 10.0 %collective-permute-start.2 = (bf16[384,384]{1,0:T(8,128)(2,1)S(1)}, bf16[384,384]{1,0:T(8,128)(2,1)S(1)}, u32[]{:S(2)}, u32[]{:S(2)}) collective-permute-start(bf16[384,384]{1,0:T(8,128)(2,1)S(1)} %pad_maximum_fusion.4), channel_id=1, source_target_pairs={{0,64},{64,128},{128,192},{192,256},{256,320},{320,384},{384,448},... | collective-permute-start | bytes 884744 | tf_op jit(solution)/shard_map/ppermute | solution.py:18
  112.7 7.1 %collective-permute-start.5 = (bf16[1536,384]{1,0:T(8,128)(2,1)S(1)}, bf16[1536,384]{1,0:T(8,128)(2,1)S(1)}, u32[]{:S(2)}, u32[]{:S(2)}) collective-permute-start(bf16[1536,384]{1,0:T(8,128)(2,1)S(1)} %bitcast.179), channel_id=1, source_target_pairs={{0,1},{1,0},{2,3},{3,2},{4,5},{5,4},{6,7},{7,6},{8,9},{9,8},{10,11... | collective-permute-start | bytes 3538952 | tf_op jit(solution)/shard_map/ppermute | solution.py:30
  121.7 11.3 %all-to-all-start.1 = ((bf16[4,32,1536]{2,1,0:T(8,128)(2,1)}), bf16[4,32,1536]{2,1,0:T(8,128)(2,1)S(1)}, u32[]{:S(2)}, u32[]{:S(2)}) async-start(bf16[4,32,1536]{2,1,0:T(8,128)(2,1)} %bitcast.49), calls=%async_computation.1 | async-start | bytes 786432 | tf_op jit(solution)/shard_map/all_to_all | solution.py:62
  135.3 9.7 %all-to-all-start.2 = ((bf16[4,32,1536]{2,1,0:T(8,128)(2,1)}), bf16[4,32,1536]{2,1,0:T(8,128)(2,1)S(1)}, u32[]{:S(2)}, u32[]{:S(2)}) async-start(bf16[4,32,1536]{2,1,0:T(8,128)(2,1)} %broadcast_in_dim.53), calls=%async_computation.2 | async-start | bytes 786432 | tf_op jit(solution)/shard_map/all_to_all | solution.py:55
  159.0 9.7 %all-to-all-start.3 = ((bf16[4,32,1536]{2,1,0:T(8,128)(2,1)}), bf16[4,32,1536]{2,1,0:T(8,128)(2,1)S(1)}, u32[]{:S(2)}, u32[]{:S(2)}) async-start(bf16[4,32,1536]{2,1,0:T(8,128)(2,1)} %bitcast.88), calls=%async_computation.3 | async-start | bytes 786432 | tf_op jit(solution)/shard_map/all_to_all | solution.py:62
  (4 other events, 69.7 us)
Sparse Core Ops, SparseCore 0:
  53.8 69.9 all-gather.1

commit v2 on v1

--- a/solution.py
+++ b/solution.py
@@ -1,6 +1,8 @@
 import jax
 import jax.numpy as jnp
 from jax import lax
+from jax.experimental import pallas as pl
+from jax.experimental.pallas import tpu as pltpu
 from jax.sharding import Mesh
 from jax.sharding import PartitionSpec as P
 
@@ -11,6 +13,8 @@
 EPS = 1e-06
 F32 = jnp.float32
 BF16 = jnp.bfloat16
+LANES = 128
+BLOCK_ROWS = 512
 
 
 def from_ahead(x, steps):
@@ -28,6 +32,81 @@
 
 def other_core(x):
     return lax.ppermute(x, "core", [(0, 1), (1, 0)])
+
+
+def ffn_kernel(x_ref, extra_ref, weights_ref, out_ref, held, arrived, *, main, tail):
+    tokens, d = x_ref.shape
+    blocks = d // BLOCK_ROWS
+    copies = []
+    for i in range(2 * blocks):
+        rows = pl.ds(i * BLOCK_ROWS, BLOCK_ROWS)
+        copies.append(pltpu.make_async_copy(weights_ref.at[rows], held.at[rows], arrived.at[i]))
+        copies[-1].start()
+    row = lax.broadcasted_iota(jnp.int32, (tokens, LANES), 0)
+    lane = lax.broadcasted_iota(jnp.int32, (tokens, LANES), 1)
+
+    def hidden_of(linear, gated, extra):
+        linear, gated = linear.astype(BF16).astype(F32), gated.astype(BF16).astype(F32)
+        before = jnp.where(row == 0, 0.0, pltpu.roll(gated, 1, 0))
+        after = jnp.where(row == tokens - 1, 0.0, pltpu.roll(gated, tokens - 1, 0))
+        mixed = extra[0:1] * before + extra[1:2] * gated + extra[2:3] * after + extra[3:4]
+        return jax.nn.gelu(mixed, approximate=True) * linear
+
+    total = jnp.zeros((tokens, d), F32)
+    for core in range(2):
+        up = jnp.zeros((tokens, 2 * main), F32)
+        tails = jnp.zeros((tokens, LANES), F32)
+        for k in range(blocks):
+            copies[core * blocks + k].wait()
+            x = x_ref[:, k * BLOCK_ROWS : (k + 1) * BLOCK_ROWS]
+            rows = pl.ds((core * blocks + k) * BLOCK_ROWS, BLOCK_ROWS)
+            up += jnp.dot(x, held[rows, : 2 * main], preferred_element_type=F32)
+            tails += jnp.dot(x, held[rows, 3 * main :], preferred_element_type=F32)
+        rows = pl.ds(core * d, d)
+        for at in range(0, main, 2 * LANES):
+            parts = []
+            for j in range(at, at + 2 * LANES, LANES):
+                extra = extra_ref[core, :, j : j + LANES]
+                parts.append(
+                    hidden_of(up[:, j : j + LANES], up[:, main + j : main + j + LANES], extra)
+                )
+            hidden = jnp.concatenate(parts, axis=1).astype(BF16)
+            total += lax.dot_general(
+                hidden,
+                held[rows, 2 * main + at : 2 * main + at + 2 * LANES],
+                (((1,), (1,)), ((), ())),
+                preferred_element_type=F32,
+            )
+        gated = pltpu.roll(tails, LANES - tail, 1)
+        hidden = hidden_of(tails, gated, extra_ref[core, :, main : main + LANES])
+        hidden = pltpu.roll(jnp.where(lane < tail, hidden, 0.0), 2 * tail, 1).astype(BF16)
+        total += lax.dot_general(
+            hidden, held[rows, 3 * main :], (((1,), (1,)), ((), ())), preferred_element_type=F32
+        )
+    out_ref[...] = total.astype(BF16)
+
+
+def ffn(x, extra, weights, main, tail):
+    tokens, d = x.shape
+    return pl.pallas_call(
+        lambda *refs: ffn_kernel(*refs, main=main, tail=tail),
+        out_shape=jax.ShapeDtypeStruct((tokens, d), BF16),
+        in_specs=[
+            pl.BlockSpec(memory_space=pltpu.VMEM),
+            pl.BlockSpec(memory_space=pltpu.VMEM),
+            pl.BlockSpec(memory_space=pltpu.HBM),
+        ],
+        out_specs=pl.BlockSpec(memory_space=pltpu.VMEM),
+        scratch_shapes=[
+            pltpu.VMEM(weights.shape, BF16),
+            pltpu.SemaphoreType.DMA((2 * d // BLOCK_ROWS,)),
+        ],
+        compiler_params=pltpu.CompilerParams(vmem_limit_bytes=55 * 1024 * 1024),
+        cost_estimate=pl.CostEstimate(
+            flops=2 * tokens * weights.size, bytes_accessed=2 * weights.size, transcendentals=0
+        ),
+        name="ffn",
+    )(x, extra, weights)
 
 
 def norm_scale(values, gain):
@@ -87,19 +166,29 @@
     d = stream.shape[1]
     core = lax.axis_index("core")
 
-    ffn_cols = jnp.concatenate([w_linear, w_gated, w_down.T], axis=1)
-    ffn_part, offsets = doubled(ffn_cols, [0], (4, 2, 1), 1)
+    main = hidden_w // (2 * LANES) * (2 * LANES)
+    tail = hidden_w - main
+    pieces = [w_linear, w_gated, w_down.T]
+    spare = jnp.zeros((rows, LANES - 3 * tail), BF16)
+    ffn_cols = jnp.concatenate(
+        [p[:, :main] for p in pieces] + [p[:, main:] for p in pieces] + [spare], axis=1
+    )
+    ffn_part, offsets = doubled(ffn_cols, [0], (4,), 1)
+    cut = ffn_cols.shape[1] // (2 * LANES) * LANES
+    left = from_ahead(ffn_part[:, :cut], 2)
+    right = from_ahead(ffn_part[:, cut:], -2)
+    right = jnp.concatenate([right[rows:], right[:rows]], axis=0)
+    ffn_part = jnp.concatenate([ffn_part, jnp.concatenate([left, right], axis=1)], axis=0)
+    ffn_part, offsets = doubled(ffn_part, offsets + [2, 6], (1,), 1)
     ffn_full = lax.all_gather(ffn_part, ("core", "fs_1"), axis=0, tiled=True)
-    ffn_full = [ffn_full[:d], ffn_full[d:]]
 
     mix_cols = jnp.concatenate([w_outer_gate, w_inner_gate, w_value, w_mix_out.T], axis=1)
     mix_part = sent_to_all(mix_cols, "fs_1")
-    mix_part, near = doubled(mix_part, [0], (4,), -1)
-    mix_part = mix_part.reshape(len(near), 2, -1, mix_part.shape[1])
     ways = []
+    half_rows = mix_part.shape[0] // 2
     for way, sign in ((0, -1), (1, 1)):
-        mine = mix_part[:, way].reshape(-1, mix_part.shape[3])
-        mine, back = doubled(mine, near, (2, 1), sign)
+        mine = mix_part[way * half_rows : (way + 1) * half_rows]
+        mine, back = doubled(mine, [0], (4, 2, 1), sign)
         mine = mine.reshape(n0, n1 // 2, rows, -1)
         ways.append(jnp.stack([mine[back.index(o)] for o in offsets], axis=1))
     mix_own = jnp.concatenate(ways, axis=0).reshape(d, -1)
@@ -108,9 +197,10 @@
     small = jnp.concatenate(
         [ffn_taps, ffn_bias[None], jnp.pad(mix_taps, ((0, 0), (0, hidden_w - width)))], axis=0
     )
+    small = jnp.pad(small, ((0, 0), (0, main + LANES - hidden_w)))
     small = [small, other_core(small)]
     mix_taps = [s[4:7, :width] for s in small]
-    small = [jnp.where(core == 0, small[0], small[1]), jnp.where(core == 0, small[1], small[0])]
+    extra = jnp.where(core == 0, jnp.stack(small), jnp.stack(small[::-1]))[:, :4]
 
     place = jnp.arange(d)
     k = place // rows % n0
@@ -143,13 +233,7 @@
     middle = middle.astype(BF16).astype(F32)
     normed_two = sent_to_all(norm_scale(middle, turned(ffn_pre_gain)).astype(BF16), "x")
 
-    partial_two = 0.0
-    for weights, extra in zip(ffn_full, small):
-        both = dot(normed_two, weights[:, : 2 * hidden_w]).astype(BF16).astype(F32)
-        linear, gated = both[:, :hidden_w], both[:, hidden_w:]
-        activated = jax.nn.gelu(conv_three(gated, extra[:3]) + extra[3], approximate=True)
-        hidden = (activated * linear).astype(BF16)
-        partial_two = partial_two + dot_t(hidden, weights[:, 2 * hidden_w :])
+    partial_two = ffn(normed_two, extra, ffn_full, main, tail)
     branch_two = rows_summed(partial_two)
     result = (middle + norm_scale(branch_two, turned(ffn_post_gain))).astype(BF16)
     result = sent_to_all(dot_t(result, chosen).astype(BF16), "x")

time: 195 us -> 192 us (0.985)
  matrix products: 22.8 us -> 8.82 us
  Pallas kernels: 0 us -> 7.09 us
  waiting for transfers between devices: 41.7 us -> 36.1 us
  starting transfers between devices: 92.2 us -> 96.4 us
  local copies, waits for them, and re-layouts: 4.87 us -> 8.99 us
    pallas_call x0 -> x1, Pallas kernels: none -> 7.09 us  [ffn(): pl.pallas_call(lambda *refs: ffn_kernel(*refs, main=main, tail=tail), out...]
    dot_general x5 -> x3, matrix products: 10.8 us -> 3.75 us  [dot_t(): lax.dot_general(a, b, (((1,), (1,)), ((), ())), preferred_element_type=F32)]
    dot_general x5 -> x3, matrix products: 12 us -> 5.07 us  [dot(): return jnp.dot(a, b, preferred_element_type=F32)]
    ppermute x2, starting transfers between devices: 10.5 us -> 17.1 us  [other_core(): return lax.ppermute(x, 'core', [(0, 1), (1, 0)])]
    ppermute x8 -> x10, waiting for transfers between devices: 22.6 us -> 16.9 us  [from_ahead(): lax.ppermute(x, ('rep', 'fs_0'), [(i, (i - steps) % n) for i in range(n)])]
    slice x2 -> x8, local copies, waits for them, and re-layouts: 0.09 us -> 4.39 us  [the longest x3 2.29 us: layer(): p[:, :main]]
    ppermute x8 -> x10, starting transfers between devices: 67.2 us -> 63.7 us  [from_ahead(): lax.ppermute(x, ('rep', 'fs_0'), [(i, (i - steps) % n) for i in range(n)])]
  transfers between devices with their start and end apart: 15 -> 17, of which waited for: 9 -> 11; matrix products, arithmetic and copies ran while one was open for 6% -> 6% of each run, Pallas kernels for 0% -> 0%
where the time goes in v2:
time: 192 us; the launch traced here: 191 us
  starting transfers between devices  96.4 us (50%)
  waiting for transfers between devices  36.1 us (19%)
  blocking collectives  15.5 us (8%)
  between operations  14.1 us (7%)
  local copies, waits for them, and re-layouts  8.99 us (5%)
  matrix products  8.82 us (5%)
  Pallas kernels  7.09 us (4%)
  other arithmetic  3.63 us (2%)
    ppermute x10, starting transfers between devices, from_ahead(): lax.ppermute(x, ('rep', 'fs_0'), [(i, (i - steps) % n) for i in range(n)])  63.7 us
    ppermute x2, starting transfers between devices, other_core(): return lax.ppermute(x, 'core', [(0, 1), (1, 0)])  17.1 us
    ppermute x10, waiting for transfers between devices, from_ahead(): lax.ppermute(x, ('rep', 'fs_0'), [(i, (i - steps) % n) for i in range(n)])  16.9 us
    all_to_all x2, waiting for transfers between devices, rows_summed(): lax.all_to_all(tiles, 'x', split_axis=0, concat_axis=0, tiled=True)  13.4 us
    all_to_all x1, blocking collectives, sent_to_all(): lax.all_to_all(jnp.broadcast_to(x[None], (n, *x.shape)), axis, 0, 0, tile...  8.62 us
    all_to_all x2, starting transfers between devices, sent_to_all(): lax.all_to_all(jnp.broadcast_to(x[None], (n, *x.shape)), axis, 0, 0, tile...  8.07 us
    all_to_all x2, starting transfers between devices, rows_summed(): lax.all_to_all(tiles, 'x', split_axis=0, concat_axis=0, tiled=True)  7.5 us
    pallas_call x1, Pallas kernels, ffn(): pl.pallas_call(lambda *refs: ffn_kernel(*refs, main=main, tail=tail), out...  7.09 us
  transfers between devices with their start and end apart: 17, of which 11 were waited for; matrix products, arithmetic and copies ran while one was open for 6% of the time, Pallas kernels for 0%

profile of v2, /device:TPU:1, one launch (start us, length us, event | category | flops | bytes accessed | tf_op | source)
XLA Modules:
  0.0 190.6 jit_solution(5667180362917148769)
XLA Ops:
  11.0 18.7 %collective-permute-start.8 = (bf16[24,1664]{1,0:T(8,128)(2,1)S(1)}, bf16[24,1664]{1,0:T(8,128)(2,1)S(1)}, u32[]{:S(2)}, u32[]{:S(2)}) collective-permute-start(bf16[24,1664]{1,0:T(8,128)(2,1)S(1)} %concatenate.69), channel_id=1, source_target_pairs={{0,768},{64,832},{128,896},{192,960},{256,0},{320,64},{384,128},{4... | collective-permute-start | bytes 239624 | tf_op jit(solution)/shard_map/ppermute | solution.py:22
  31.2 4.0 %collective-permute-start.10 = (bf16[48,896]{1,0:T(8,128)(2,1)S(1)}, bf16[48,896]{1,0:T(8,128)(2,1)S(1)}, u32[]{:S(2)}, u32[]{:S(2)}) collective-permute-start(bf16[48,896]{1,0:T(8,128)(2,1)S(1)} %pad_maximum_fusion.6), channel_id=1, source_target_pairs={{0,128},{64,192},{128,256},{192,320},{256,384},{320,448},{384,512}... | collective-permute-start | bytes 258056 | tf_op jit(solution)/shard_map/ppermute | solution.py:22
  35.2 5.7 %collective-permute-start.9 = (bf16[48,768]{1,0:T(8,128)(2,1)S(1)}, bf16[48,768]{1,0:T(8,128)(2,1)S(1)}, u32[]{:S(2)}, u32[]{:S(2)}) collective-permute-start(bf16[48,768]{1,0:T(8,128)(2,1)S(1)} %pad_maximum_fusion.7), channel_id=1, source_target_pairs={{0,896},{64,960},{128,0},{192,64},{256,128},{320,192},{384,256},{4... | collective-permute-start | bytes 221192 | tf_op jit(solution)/shard_map/ppermute | solution.py:22
  42.4 7.9 %collective-permute-start.11 = (bf16[96,1664]{1,0:T(8,128)(2,1)S(1)}, bf16[96,1664]{1,0:T(8,128)(2,1)S(1)}, u32[]{:S(2)}, u32[]{:S(2)}) collective-permute-start(bf16[96,1664]{1,0:T(8,128)(2,1)S(1)} %maximum_maximum_fusion), channel_id=1, source_target_pairs={{0,960},{64,0},{128,64},{192,128},{256,192},{320,256},{384,320},{4... | collective-permute-start | bytes 958472 | tf_op jit(solution)/shard_map/ppermute | solution.py:22
  50.4 4.2 %collective-permute-done.11 = bf16[96,1664]{1,0:T(8,128)(2,1)S(1)} collective-permute-done((bf16[96,1664]{1,0:T(8,128)(2,1)S(1)}, bf16[96,1664]{1,0:T(8,128)(2,1)S(1)}, u32[]{:S(2)}, u32[]{:S(2)}) %collective-permute-start.11) | collective-permute-done | bytes 319520 | tf_op jit(solution)/shard_map/ppermute | solution.py:22
  56.2 4.6 %all-to-all-start = ((bf16[8,24,384]{2,1,0:T(8,128)(2,1)}), bf16[8,24,384]{2,1,0:T(8,128)(2,1)S(1)}, u32[]{:S(2)}, u32[]{:S(2)}) async-start(bf16[8,24,384]{2,1,0:T(8,128)(2,1)} %broadcast_in_dim.54), calls=%async_computation | async-start | bytes 294912 | tf_op jit(solution)/shard_map/all_to_all | solution.py:134
  60.9 7.8 %collective-permute-start.7 = (f32[7,640]{1,0:T(8,128)S(1)}, f32[7,640]{1,0:T(8,128)S(1)}, u32[]{:S(2)}, u32[]{:S(2)}) collective-permute-start(f32[7,640]{1,0:T(8,128)S(1)} %get-tuple-element.56), channel_id=1, source_target_pairs={{0,1},{1,0},{2,3},{3,2},{4,5},{5,4},{6,7},{7,6},{8,9},{9,8},{10,11... | collective-permute-start | bytes 53768 | tf_op jit(solution)/shard_map/ppermute | solution.py:34
  69.1 2.9 %fusion.23 = (f32[128]{0:T(128)S(1)}, bf16[128,1536]{1,0:T(8,128)(2,1)}) fusion(s32[1536]{0:T(1024)S(1)} %fusion.82, bf16[256,1536]{1,0:T(8,128)(2,1)S(1)} %copy-done, s32[]{:T(128)S(6)} %select_n.114), kind=kOutput, calls=%fused_computation.20 | convolution fusion | flops 607125376 | bytes 795140 | tf_op jit(solution)/shard_map/dot_general | solution.py:125
  72.0 7.8 %collective-permute-start.3 = (bf16[96,384]{1,0:T(8,128)(2,1)S(1)}, bf16[96,384]{1,0:T(8,128)(2,1)S(1)}, u32[]{:S(2)}, u32[]{:S(2)}) collective-permute-start(bf16[96,384]{1,0:T(8,128)(2,1)S(1)} %bitcast.165), channel_id=1, source_target_pairs={{0,768},{64,832},{128,896},{192,960},{256,0},{320,64},{384,128},{4... | collective-permute-start | bytes 221192 | tf_op jit(solution)/shard_map/ppermute | solution.py:22
  82.8 5.7 %collective-permute-start.4 = (bf16[192,384]{1,0:T(8,128)(2,1)S(1)}, bf16[192,384]{1,0:T(8,128)(2,1)S(1)}, u32[]{:S(2)}, u32[]{:S(2)}) collective-permute-start(bf16[192,384]{1,0:T(8,128)(2,1)S(1)} %pad_maximum_fusion.5), channel_id=1, source_target_pairs={{0,896},{64,960},{128,0},{192,64},{256,128},{320,192},{384,256},{4... | collective-permute-start | bytes 442376 | tf_op jit(solution)/shard_map/ppermute | solution.py:22
  88.8 2.9 %collective-permute-start.1 = (bf16[192,384]{1,0:T(8,128)(2,1)S(1)}, bf16[192,384]{1,0:T(8,128)(2,1)S(1)}, u32[]{:S(2)}, u32[]{:S(2)}) collective-permute-start(bf16[192,384]{1,0:T(8,128)(2,1)S(1)} %pad_maximum_fusion.4), channel_id=1, source_target_pairs={{0,128},{64,192},{128,256},{192,320},{256,384},{320,448},{384,512}... | collective-permute-start | bytes 442376 | tf_op jit(solution)/shard_map/ppermute | solution.py:22
  92.1 5.4 %collective-permute-start.5 = (bf16[384,384]{1,0:T(8,128)(2,1)S(1)}, bf16[384,384]{1,0:T(8,128)(2,1)S(1)}, u32[]{:S(2)}, u32[]{:S(2)}) collective-permute-start(bf16[384,384]{1,0:T(8,128)(2,1)S(1)} %pad_maximum_fusion.3), channel_id=1, source_target_pairs={{0,960},{64,0},{128,64},{192,128},{256,192},{320,256},{384,320},{4... | collective-permute-start | bytes 884744 | tf_op jit(solution)/shard_map/ppermute | solution.py:22
  99.1 3.7 %collective-permute-start.2 = (bf16[384,384]{1,0:T(8,128)(2,1)S(1)}, bf16[384,384]{1,0:T(8,128)(2,1)S(1)}, u32[]{:S(2)}, u32[]{:S(2)}) collective-permute-start(bf16[384,384]{1,0:T(8,128)(2,1)S(1)} %pad_maximum_fusion.2), channel_id=1, source_target_pairs={{0,64},{64,128},{128,192},{192,256},{256,320},{320,384},{384,448},... | collective-permute-start | bytes 884744 | tf_op jit(solution)/shard_map/ppermute | solution.py:22
  103.0 6.7 %collective-permute-done.2 = bf16[384,384]{1,0:T(8,128)(2,1)S(1)} collective-permute-done((bf16[384,384]{1,0:T(8,128)(2,1)S(1)}, bf16[384,384]{1,0:T(8,128)(2,1)S(1)}, u32[]{:S(2)}, u32[]{:S(2)}) %collective-permute-start.2) | collective-permute-done | bytes 294944 | tf_op jit(solution)/shard_map/ppermute | solution.py:22
  110.0 9.3 %collective-permute-start.6 = (bf16[1536,384]{1,0:T(8,128)(2,1)S(1)}, bf16[1536,384]{1,0:T(8,128)(2,1)S(1)}, u32[]{:S(2)}, u32[]{:S(2)}) collective-permute-start(bf16[1536,384]{1,0:T(8,128)(2,1)S(1)} %bitcast.154), channel_id=1, source_target_pairs={{0,1},{1,0},{2,3},{3,2},{4,5},{5,4},{6,7},{7,6},{8,9},{9,8},{10,11... | collective-permute-start | bytes 3538952 | tf_op jit(solution)/shard_map/ppermute | solution.py:34
  124.0 4.0 %all-to-all-start.1 = ((bf16[4,32,1536]{2,1,0:T(8,128)(2,1)}), bf16[4,32,1536]{2,1,0:T(8,128)(2,1)S(1)}, u32[]{:S(2)}, u32[]{:S(2)}) async-start(bf16[4,32,1536]{2,1,0:T(8,128)(2,1)} %bitcast.47), calls=%async_computation.1 | async-start | bytes 786432 | tf_op jit(solution)/shard_map/all_to_all | solution.py:141
  128.2 7.4 %all-to-all-done.1 = bf16[4,32,1536]{2,1,0:T(8,128)(2,1)S(1)} async-done(((bf16[4,32,1536]{2,1,0:T(8,128)(2,1)}), bf16[4,32,1536]{2,1,0:T(8,128)(2,1)S(1)}, u32[]{:S(2)}, u32[]{:S(2)}) %all-to-all-start.1) | async-done | bytes 393248 | tf_op jit(solution)/shard_map/all_to_all | solution.py:141
  137.8 3.5 %all-to-all-start.2 = ((bf16[4,32,1536]{2,1,0:T(8,128)(2,1)}), bf16[4,32,1536]{2,1,0:T(8,128)(2,1)S(1)}, u32[]{:S(2)}, u32[]{:S(2)}) async-start(bf16[4,32,1536]{2,1,0:T(8,128)(2,1)} %broadcast_in_dim.56), calls=%async_computation.2 | async-start | bytes 786432 | tf_op jit(solution)/shard_map/all_to_all | solution.py:134
  141.9 5.8 %all-to-all-done.2 = bf16[4,32,1536]{2,1,0:T(8,128)(2,1)S(1)} async-done(((bf16[4,32,1536]{2,1,0:T(8,128)(2,1)}), bf16[4,32,1536]{2,1,0:T(8,128)(2,1)S(1)}, u32[]{:S(2)}, u32[]{:S(2)}) %all-to-all-start.2) | async-done | bytes 393248 | tf_op jit(solution)/shard_map/all_to_all | solution.py:134
  148.4 7.1 %ffn.1 = bf16[128,1536]{1,0:T(8,128)(2,1)} custom-call(bf16[128,1536]{1,0:T(8,128)(2,1)} %bitcast.158, f32[2,4,640]{2,1,0:T(4,128)} %fusion.71.refs_1_, bf16[3072,1664]{1,0:T(8,128)(2,1)} %all-gather.2.cloned.1.call-done.refs_2_), custom_call_target="tpu_custom_call" | custom-call | flops 1308622848 | bytes 10223616 | tf_op jit(solution)/shard_map/ffn/pallas_call | solution.py:91
  155.5 3.5 %all-to-all-start.3 = ((bf16[4,32,1536]{2,1,0:T(8,128)(2,1)}), bf16[4,32,1536]{2,1,0:T(8,128)(2,1)S(1)}, u32[]{:S(2)}, u32[]{:S(2)}) async-start(bf16[4,32,1536]{2,1,0:T(8,128)(2,1)} %bitcast.157), calls=%async_computation.3 | async-start | bytes 786432 | tf_op jit(solution)/shard_map/all_to_all | solution.py:141
  159.2 6.0 %all-to-all-done.3 = bf16[4,32,1536]{2,1,0:T(8,128)(2,1)S(1)} async-done(((bf16[4,32,1536]{2,1,0:T(8,128)(2,1)}), bf16[4,32,1536]{2,1,0:T(8,128)(2,1)S(1)}, u32[]{:S(2)}, u32[]{:S(2)}) %all-to-all-start.3) | async-done | bytes 393248 | tf_op jit(solution)/shard_map/all_to_all | solution.py:141
  167.4 8.6 %all_to_all.25 = bf16[4,32,1536]{2,1,0:T(8,128)(2,1)S(1)} all-to-all(bf16[4,32,1536]{2,1,0:T(8,128)(2,1)S(1)} %broadcast_in_dim.58), channel_id=1, replica_groups=mesh['rep'=2,'fs_0'=8,'fs_1'=8,'x'=4,'core'=2] {'x'}, dimensions={0} | all-to-all | bytes 786432 | tf_op jit(solution)/shard_map/all_to_all | solution.py:134
  176.0 6.9 %all_gather.7 = bf16[256,1536]{1,0:T(8,128)(2,1)S(1)} all-gather(bf16[128,1536]{1,0:T(8,128)(2,1)S(1)} %bitcast.159), channel_id=1, replica_groups=mesh['rep'=2,'fs_0'=8,'fs_1'=8,'x'=4,'core'=2] {'core'}, dimensions={0}, use_global_device_ids=true | all-gather | bytes 1179648 | tf_op jit(solution)/shard_map/all_gather | solution.py:240
  (129 shorter events, 26.6 us)
Async XLA Ops:
  6.5 62.5 %copy-start = (bf16[256,1536]{1,0:T(8,128)(2,1)S(1)}, bf16[256,1536]{1,0:T(8,128)(2,1)}, u32[]{:S(2)}) copy-start(bf16[256,1536]{1,0:T(8,128)(2,1)} %param.15) | copy-start | bytes 2359300
  6.5 141.2 %all-gather.2.cloned.1.call-start = ((), (), s32[]{:S(2)}) async-start(), calls=%async_computation.5 | async-start | bytes 10862592 | tf_op jit(solution)/shard_map/all_gather | solution.py:183
  11.0 20.2 %collective-permute-start.8 = (bf16[24,1664]{1,0:T(8,128)(2,1)S(1)}, bf16[24,1664]{1,0:T(8,128)(2,1)S(1)}, u32[]{:S(2)}, u32[]{:S(2)}) collective-permute-start(bf16[24,1664]{1,0:T(8,128)(2,1)S(1)} %concatenate.69), channel_id=1, source_target_pairs={{0,768},{64,832},{128,896},{192,960},{256,0},{320,64},{384,128},{4... | collective-permute-start | bytes 239624 | tf_op jit(solution)/shard_map/ppermute | solution.py:22
  31.2 9.8 %collective-permute-start.10 = (bf16[48,896]{1,0:T(8,128)(2,1)S(1)}, bf16[48,896]{1,0:T(8,128)(2,1)S(1)}, u32[]{:S(2)}, u32[]{:S(2)}) collective-permute-start(bf16[48,896]{1,0:T(8,128)(2,1)S(1)} %pad_maximum_fusion.6), channel_id=1, source_target_pairs={{0,128},{64,192},{128,256},{192,320},{256,384},{320,448},{384,512}... | collective-permute-start | bytes 258056 | tf_op jit(solution)/shard_map/ppermute | solution.py:22
  35.2 7.1 %collective-permute-start.9 = (bf16[48,768]{1,0:T(8,128)(2,1)S(1)}, bf16[48,768]{1,0:T(8,128)(2,1)S(1)}, u32[]{:S(2)}, u32[]{:S(2)}) collective-permute-start(bf16[48,768]{1,0:T(8,128)(2,1)S(1)} %pad_maximum_fusion.7), channel_id=1, source_target_pairs={{0,896},{64,960},{128,0},{192,64},{256,128},{320,192},{384,256},{4... | collective-permute-start | bytes 221192 | tf_op jit(solution)/shard_map/ppermute | solution.py:22
  42.3 13.1 %copy-start.12 = (bf16[24,96]{1,0:T(8,128)(2,1)S(1)}, bf16[24,96]{1,0:T(8,128)(2,1)}, u32[]{:S(2)}) copy-start(bf16[24,96]{1,0:T(8,128)(2,1)} %param.17) | copy-start | bytes 13828
  42.4 18.5 %copy-start.13 = (f32[528]{0:T(1024)S(1)}, f32[528]{0:T(1024)}, u32[]{:S(2)}) copy-start(f32[528]{0:T(1024)} %param.27) | copy-start | bytes 6340
  42.4 18.5 %copy-start.3 = (f32[3,528]{1,0:T(4,128)S(1)}, f32[3,528]{1,0:T(4,128)}, u32[]{:S(2)}) copy-start(f32[3,528]{1,0:T(4,128)} %param.26) | copy-start | bytes 19012
  42.4 18.5 %copy-start.8 = (f32[3,96]{1,0:T(4,128)S(1)}, f32[3,96]{1,0:T(4,128)}, u32[]{:S(2)}) copy-start(f32[3,96]{1,0:T(4,128)} %param.20) | copy-start | bytes 3460
  42.4 26.3 %copy-start.4 = (f32[1536]{0:T(1024)S(1)}, f32[1536]{0:T(1024)}, u32[]{:S(2)}) copy-start(f32[1536]{0:T(1024)} %param.22) | copy-start | bytes 18436
  42.4 26.4 %copy-start.5 = (f32[1536]{0:T(1024)S(1)}, f32[1536]{0:T(1024)}, u32[]{:S(2)}) copy-start(f32[1536]{0:T(1024)} %param.16) | copy-start | bytes 18436
  42.4 12.1 %collective-permute-start.11 = (bf16[96,1664]{1,0:T(8,128)(2,1)S(1)}, bf16[96,1664]{1,0:T(8,128)(2,1)S(1)}, u32[]{:S(2)}, u32[]{:S(2)}) collective-permute-start(bf16[96,1664]{1,0:T(8,128)(2,1)S(1)} %maximum_maximum_fusion), channel_id=1, source_target_pairs={{0,960},{64,0},{128,64},{192,128},{256,192},{320,256},{384,320},{4... | collective-permute-start | bytes 958472 | tf_op jit(solution)/shard_map/ppermute | solution.py:22
  56.2 15.7 %all-to-all-start = ((bf16[8,24,384]{2,1,0:T(8,128)(2,1)}), bf16[8,24,384]{2,1,0:T(8,128)(2,1)S(1)}, u32[]{:S(2)}, u32[]{:S(2)}) async-start(bf16[8,24,384]{2,1,0:T(8,128)(2,1)} %broadcast_in_dim.54), calls=%async_computation | async-start | bytes 294912 | tf_op jit(solution)/shard_map/all_to_all | solution.py:134
  60.9 58.9 %collective-permute-start.7 = (f32[7,640]{1,0:T(8,128)S(1)}, f32[7,640]{1,0:T(8,128)S(1)}, u32[]{:S(2)}, u32[]{:S(2)}) collective-permute-start(f32[7,640]{1,0:T(8,128)S(1)} %get-tuple-element.56), channel_id=1, source_target_pairs={{0,1},{1,0},{2,3},{3,2},{4,5},{5,4},{6,7},{7,6},{8,9},{9,8},{10,11... | collective-permute-start | bytes 53768 | tf_op jit(solution)/shard_map/ppermute | solution.py:34
  72.0 10.8 %collective-permute-start.3 = (bf16[96,384]{1,0:T(8,128)(2,1)S(1)}, bf16[96,384]{1,0:T(8,128)(2,1)S(1)}, u32[]{:S(2)}, u32[]{:S(2)}) collective-permute-start(bf16[96,384]{1,0:T(8,128)(2,1)S(1)} %bitcast.165), channel_id=1, source_target_pairs={{0,768},{64,832},{128,896},{192,960},{256,0},{320,64},{384,128},{4... | collective-permute-start | bytes 221192 | tf_op jit(solution)/shard_map/ppermute | solution.py:22
  79.8 9.0 %collective-permute-start = (bf16[96,384]{1,0:T(8,128)(2,1)S(1)}, bf16[96,384]{1,0:T(8,128)(2,1)S(1)}, u32[]{:S(2)}, u32[]{:S(2)}) collective-permute-start(bf16[96,384]{1,0:T(8,128)(2,1)S(1)} %bitcast.162), channel_id=1, source_target_pairs={{0,256},{64,320},{128,384},{192,448},{256,512},{320,576},{384,640}... | collective-permute-start | bytes 221192 | tf_op jit(solution)/shard_map/ppermute | solution.py:22
  82.8 9.3 %collective-permute-start.4 = (bf16[192,384]{1,0:T(8,128)(2,1)S(1)}, bf16[192,384]{1,0:T(8,128)(2,1)S(1)}, u32[]{:S(2)}, u32[]{:S(2)}) collective-permute-start(bf16[192,384]{1,0:T(8,128)(2,1)S(1)} %pad_maximum_fusion.5), channel_id=1, source_target_pairs={{0,896},{64,960},{128,0},{192,64},{256,128},{320,192},{384,256},{4... | collective-permute-start | bytes 442376 | tf_op jit(solution)/shard_map/ppermute | solution.py:22
  88.8 10.3 %collective-permute-start.1 = (bf16[192,384]{1,0:T(8,128)(2,1)S(1)}, bf16[192,384]{1,0:T(8,128)(2,1)S(1)}, u32[]{:S(2)}, u32[]{:S(2)}) collective-permute-start(bf16[192,384]{1,0:T(8,128)(2,1)S(1)} %pad_maximum_fusion.4), channel_id=1, source_target_pairs={{0,128},{64,192},{128,256},{192,320},{256,384},{320,448},{384,512}... | collective-permute-start | bytes 442376 | tf_op jit(solution)/shard_map/ppermute | solution.py:22
  92.1 10.8 %collective-permute-start.5 = (bf16[384,384]{1,0:T(8,128)(2,1)S(1)}, bf16[384,384]{1,0:T(8,128)(2,1)S(1)}, u32[]{:S(2)}, u32[]{:S(2)}) collective-permute-start(bf16[384,384]{1,0:T(8,128)(2,1)S(1)} %pad_maximum_fusion.3), channel_id=1, source_target_pairs={{0,960},{64,0},{128,64},{192,128},{256,192},{320,256},{384,320},{4... | collective-permute-start | bytes 884744 | tf_op jit(solution)/shard_map/ppermute | solution.py:22
  99.1 10.6 %collective-permute-start.2 = (bf16[384,384]{1,0:T(8,128)(2,1)S(1)}, bf16[384,384]{1,0:T(8,128)(2,1)S(1)}, u32[]{:S(2)}, u32[]{:S(2)}) collective-permute-start(bf16[384,384]{1,0:T(8,128)(2,1)S(1)} %pad_maximum_fusion.2), channel_id=1, source_target_pairs={{0,64},{64,128},{128,192},{192,256},{256,320},{320,384},{384,448},... | collective-permute-start | bytes 884744 | tf_op jit(solution)/shard_map/ppermute | solution.py:22
  110.0 12.0 %collective-permute-start.6 = (bf16[1536,384]{1,0:T(8,128)(2,1)S(1)}, bf16[1536,384]{1,0:T(8,128)(2,1)S(1)}, u32[]{:S(2)}, u32[]{:S(2)}) collective-permute-start(bf16[1536,384]{1,0:T(8,128)(2,1)S(1)} %bitcast.154), channel_id=1, source_target_pairs={{0,1},{1,0},{2,3},{3,2},{4,5},{5,4},{6,7},{7,6},{8,9},{9,8},{10,11... | collective-permute-start | bytes 3538952 | tf_op jit(solution)/shard_map/ppermute | solution.py:34
  124.0 11.6 %all-to-all-start.1 = ((bf16[4,32,1536]{2,1,0:T(8,128)(2,1)}), bf16[4,32,1536]{2,1,0:T(8,128)(2,1)S(1)}, u32[]{:S(2)}, u32[]{:S(2)}) async-start(bf16[4,32,1536]{2,1,0:T(8,128)(2,1)} %bitcast.47), calls=%async_computation.1 | async-start | bytes 786432 | tf_op jit(solution)/shard_map/all_to_all | solution.py:141
  137.8 9.9 %all-to-all-start.2 = ((bf16[4,32,1536]{2,1,0:T(8,128)(2,1)}), bf16[4,32,1536]{2,1,0:T(8,128)(2,1)S(1)}, u32[]{:S(2)}, u32[]{:S(2)}) async-start(bf16[4,32,1536]{2,1,0:T(8,128)(2,1)} %broadcast_in_dim.56), calls=%async_computation.2 | async-start | bytes 786432 | tf_op jit(solution)/shard_map/all_to_all | solution.py:134
  155.5 9.7 %all-to-all-start.3 = ((bf16[4,32,1536]{2,1,0:T(8,128)(2,1)}), bf16[4,32,1536]{2,1,0:T(8,128)(2,1)S(1)}, u32[]{:S(2)}, u32[]{:S(2)}) async-start(bf16[4,32,1536]{2,1,0:T(8,128)(2,1)} %bitcast.157), calls=%async_computation.3 | async-start | bytes 786432 | tf_op jit(solution)/shard_map/all_to_all | solution.py:141
  (7 other events, 61.9 us)
Sparse Core Ops, SparseCore 0:
  55.5 75.3 all-gather.1
